TPU v7x, 256 devices: a whole 4x4x8 slice. The times are simulated.
256 devices in a mesh: dp: 4 (over x), kv: 32 (over z, y), tp: 2 (over core).
Axes of the slice: x: 4, y: 4, z: 8, core: 2. Of those that a mesh axis runs over, the one named last changes fastest.
Arguments:
- tokens: bfloat16 [64, 16, 4096], P('dp', None, 'kv'), may hold values from -64 to 64
- in_gain: bfloat16 [4096], P('kv'), may hold values from 0.099609375 to 1.8984375
- query_weight: bfloat16 [4096, 4096], P('kv', 'tp'), may hold values from -0.125 to 0.125
- key_weight: bfloat16 [4096, 4096], P('kv', 'tp'), may hold values from -0.125 to 0.125
- value_weight: bfloat16 [4096, 4096], P('kv', 'tp'), may hold values from -0.09375 to 0.09375
- out_weight: bfloat16 [4096, 4096], P('tp', 'kv'), may hold values from -0.1875 to 0.1875
- lambdas: float32 [16], P('tp'), may hold values from 0.3 to 0.8
- sub_gain: bfloat16 [256], replicated, may hold values from 0.099609375 to 1.8984375
- key_cache: bfloat16 [64, 1024, 16, 2, 128], P('dp', 'kv', 'tp'), may hold values from -248 to 248
- value_cache: bfloat16 [64, 1024, 16, 256], P('dp', 'kv', 'tp'), may hold values from -6 to 6
- cache_len: int32 [64], P('dp'), may hold values from 512 to 992
- accepted: int32 [64], P('dp'), may hold values from 0 to 16
- parents: int32 [64, 16], P('dp'), may hold values from -1 to 14, as said below
Outputs:
- output: bfloat16 [64, 16, 4096], P('dp', None, ('kv', 'tp'))
- key_cache_out: bfloat16 [64, 1024, 16, 2, 128], P('dp', 'kv', 'tp')
- value_cache_out: bfloat16 [64, 1024, 16, 256], P('dp', 'kv', 'tp')
Inputs may be any that keep to these rules, and one draw needn't show every extreme that they name: `parents`: each proposal's parent is -1 (the text already in the cache) or one of the three proposals just before it; the last proposal's parent is the one just before it. Positions below cache_len plus accepted hold a sequence's text; the later ones are stale.
All inputs are finite; a program needn't handle non-finite values.
Results may differ from a plain program's by a relative error of at most 0.019.
The roundings to bfloat16 on the way count: a program that leaves them out, or rounds other values in their place, can miss the bound.
Values may be sent and summed in bfloat16 or wider, within the bound.
A program may use at most 64 MiB of HBM per device.

v0:
```python
import math

import jax
import jax.numpy as jnp
from jax import lax
from jax.sharding import Mesh
from jax.sharding import PartitionSpec as P

D = 4096
KV = ("kv_0", "kv_1")
KV_TP = ("kv_0", "kv_1", "tp")


LAMBDA_SCALE = 0.2 + 0.6 * math.exp(-0.6)
NEG_FILL = -1e30


def sent_to_all(value, axis):
    size = lax.axis_size(axis)
    return lax.all_to_all(
        jnp.broadcast_to(value[None], (size, *value.shape)), axis, 0, 0, tiled=True
    )


def over_copies(value, axis):
    return sent_to_all(value, axis).sum(axis=0)


def gather_axes(value, axes, dim):
    for axis in reversed(axes):
        value = lax.all_gather(value, axis, axis=dim, tiled=True)
    return value


def rows_first(arrays, axis, dims):
    turned = [jnp.moveaxis(a, dim, 0) for a, dim in zip(arrays, dims)]
    widths = [t[0].size for t in turned]
    both = jnp.concatenate([t.reshape(-1, w) for t, w in zip(turned, widths)], axis=1)
    filled = lax.all_gather(both, axis, axis=0, tiled=True)
    pieces = jnp.split(filled, [sum(widths[:k]) for k in range(1, len(widths))], axis=1)
    return tuple(
        (
            jnp.moveaxis(b.reshape(-1, *t.shape[1:]), 0, dim)
            for b, t, dim in zip(pieces, turned, dims)
        )
    )


def all_in_one(value, axis):
    leaves = jax.tree.leaves(value)
    order = sorted(range(len(leaves)), key=lambda k: -leaves[k].size)
    width = (1, *leaves[order[0]].shape)[-1]
    lines = [
        jnp.pad(leaves[k].reshape(-1), (0, -leaves[k].size % width)).reshape(-1, width)
        for k in order
    ]
    both, at, found = (lax.all_gather(jnp.concatenate(lines), axis), 0, {})
    for k, line in zip(order, lines):
        share = both[:, at : at + len(line)].reshape(len(both), -1)
        found[k] = share[:, : leaves[k].size].reshape(-1, *leaves[k].shape)
        at += len(line)
    numbers = iter(range(len(leaves)))
    return jax.tree.map(lambda _: found[next(numbers)], value)


def merged_by_axis(value, axes, combine):
    for axis in axes:
        pieces = all_in_one(value, axis)
        value = jax.tree.map(lambda part: part[0], pieces)
        for k in range(1, lax.axis_size(axis)):
            value = combine(value, jax.tree.map(lambda part: part[k], pieces))
    return value


def by_axis(value, axes):
    for axis in axes:
        value = lax.psum(value, axis)
    return value


def split_up(value, dim, size):
    lengths = value.shape
    pieces = value.reshape(*lengths[:dim], size, lengths[dim] // size, *lengths[dim + 1 :])
    return jnp.moveaxis(pieces, dim, 0)


def sent_and_summed(value, axis, dim):
    pieces = split_up(value, dim, lax.axis_size(axis))
    arrived = lax.all_to_all(pieces, axis, split_axis=0, concat_axis=0, tiled=True)
    return arrived.astype(jnp.float32).sum(axis=0)


def visible_links(parents):
    number = parents.shape[-1]
    identity = jnp.eye(number, dtype=jnp.float32)
    parent_links = (parents[..., :, None] == jnp.arange(number, dtype=jnp.int32)[None, :]).astype(
        jnp.float32
    )

    def extend(repeat, reached):
        return jnp.maximum(
            identity,
            jnp.einsum("bij,bjk->bik", parent_links, reached, precision=lax.Precision.HIGHEST),
        )

    reached = lax.fori_loop(0, number, extend, jnp.broadcast_to(identity, parent_links.shape))
    depths = (jnp.sum(reached, axis=-1) - 1.0).astype(jnp.int32)
    return (reached > 0.5, depths)


def merge_stats(former, latter):
    highest = jnp.maximum(former[0], latter[0])
    totals = former[1] * jnp.exp(former[0] - highest) + latter[1] * jnp.exp(latter[0] - highest)
    return (highest, totals)


def per_device(
    tokens,
    in_gain,
    query_weight,
    key_weight,
    value_weight,
    out_weight,
    lambdas,
    sub_gain,
    key_cache,
    value_cache,
    cache_len,
    accepted,
    parents,
):
    seq_count, prop_count, width_part = tokens.shape
    heads_here = lambdas.shape[0]
    span_here = key_cache.shape[1]
    head_dim = key_cache.shape[-1]
    half_dim = head_dim // 2
    row_count = seq_count * prop_count
    tokens_wide = tokens.astype(jnp.float32)
    squares = over_copies(jnp.sum(tokens_wide * tokens_wide, axis=-1), KV)
    row_scale = lax.rsqrt(squares.reshape(row_count) / D + 1e-06)
    normed = (
        (tokens_wide * in_gain.astype(jnp.float32))
        .astype(jnp.bfloat16)
        .reshape(row_count, width_part)
    )
    starts = cache_len + accepted
    visible, depths = visible_links(parents)
    positions = (starts[:, None] + depths).reshape(row_count)

    def pair_order(weight):
        rows_here = weight.shape[0]
        return (
            weight.reshape(rows_here, 2 * heads_here, 2, half_dim)
            .transpose(0, 1, 3, 2)
            .reshape(rows_here, -1)
        )

    cols_q, cols_k, cols_v = (
        lax.all_to_all(pair_order(query_weight), KV, split_axis=1, concat_axis=0, tiled=True),
        lax.all_to_all(pair_order(key_weight), KV, split_axis=1, concat_axis=0, tiled=True),
        lax.all_to_all(value_weight, KV, split_axis=1, concat_axis=0, tiled=True),
    )
    all_normed = gather_axes(normed, KV, 1)
    pair_count = cols_q.shape[1] // 2
    first_pair = lax.axis_index(KV) * pair_count
    pair_slot = (first_pair + jnp.arange(pair_count, dtype=jnp.int32)) % half_dim
    frequency = 10000.0 ** (-pair_slot.astype(jnp.float32) / half_dim)
    angles = positions.astype(jnp.float32)[:, None] * frequency[None, :]
    cosine = jnp.cos(angles)
    sine_part = jnp.sin(angles)

    def turned(weight):
        product = (
            jnp.dot(all_normed, weight, preferred_element_type=jnp.float32) * row_scale[:, None]
        )
        pairs = product.reshape(row_count, pair_count, 2)
        lower_half = pairs[..., 0]
        upper_half = pairs[..., 1]
        result = jnp.stack(
            [
                lower_half * cosine - upper_half * sine_part,
                upper_half * cosine + lower_half * sine_part,
            ],
            axis=-1,
        )
        return result.reshape(row_count, 2 * pair_count).astype(jnp.bfloat16)

    own_q = turned(cols_q)
    own_k = turned(cols_k)
    own_v = (
        jnp.dot(all_normed, cols_v, preferred_element_type=jnp.float32) * row_scale[:, None]
    ).astype(jnp.bfloat16)
    got_q, got_k, new_values = rows_first((own_q, own_k, own_v), KV, (1, 1, 1))

    def head_order(rows):
        return (
            rows.reshape(row_count, 2 * heads_here, half_dim, 2)
            .transpose(0, 1, 3, 2)
            .reshape(row_count, -1)
        )

    queries = head_order(got_q)
    new_keys = head_order(got_k)
    query_blocks = queries.reshape(seq_count, prop_count, heads_here, 2, head_dim)
    key_blocks = new_keys.reshape(seq_count, prop_count, heads_here, 2, head_dim)
    value_blocks = new_values.reshape(seq_count, prop_count, heads_here, 2 * head_dim)
    offset = lax.axis_index(KV) * span_here
    slot_index = starts[:, None] + jnp.arange(prop_count, dtype=jnp.int32)[None, :] - offset
    slot_index = jnp.where((slot_index >= 0) & (slot_index < span_here), slot_index, span_here)
    seq_index = jnp.broadcast_to(jnp.arange(seq_count, dtype=jnp.int32)[:, None], slot_index.shape)
    key_out = key_cache.at[seq_index, slot_index].set(key_blocks, mode="drop")
    value_out = value_cache.at[seq_index, slot_index].set(value_blocks, mode="drop")
    inverse_root = head_dim ** (-0.5)
    cache_scores = (
        jnp.einsum(
            "bqhmd,bthmd->bhmqt", query_blocks, key_cache, preferred_element_type=jnp.float32
        )
        * inverse_root
    )
    live_mask = (offset + jnp.arange(span_here, dtype=jnp.int32))[None, :] < starts[:, None]
    live_mask = live_mask[:, None, None, None, :]
    cache_scores = jnp.where(live_mask, cache_scores, NEG_FILL)
    local_peak = jnp.max(cache_scores, axis=-1)
    local_total = jnp.sum(
        jnp.where(live_mask, jnp.exp(cache_scores - local_peak[..., None]), 0.0), axis=-1
    )
    cache_peak, cache_total = merged_by_axis((local_peak, local_total), KV, merge_stats)
    own_scores = (
        jnp.einsum(
            "bqhmd,bjhmd->bhmqj", query_blocks, key_blocks, preferred_element_type=jnp.float32
        )
        * inverse_root
    )
    seen_mask = visible[:, None, None]
    own_scores = jnp.where(seen_mask, own_scores, NEG_FILL)
    own_peak = jnp.max(own_scores, axis=-1)
    own_total = jnp.sum(
        jnp.where(seen_mask, jnp.exp(own_scores - own_peak[..., None]), 0.0), axis=-1
    )
    peak_all, totals = merge_stats((cache_peak, cache_total), (own_peak, own_total))
    lam_mix = lambdas[None, :, None, None]

    def weights_of(scores, alive):
        probs = jnp.where(alive, jnp.exp(scores - peak_all[..., None]), 0.0) / totals[..., None]
        return (probs[:, :, 0] - lam_mix * probs[:, :, 1]).astype(jnp.bfloat16)

    cache_weight = weights_of(cache_scores, live_mask)
    partial_value = jnp.einsum(
        "bhqt,bthe->bqhe", cache_weight, value_cache, preferred_element_type=jnp.float32
    )
    summed = by_axis(partial_value.astype(jnp.bfloat16), KV).astype(jnp.float32)
    own_weight = weights_of(own_scores, seen_mask)
    attended = summed + jnp.einsum(
        "bhqj,bjhe->bqhe", own_weight, value_blocks, preferred_element_type=jnp.float32
    )
    mixed_out = attended * lax.rsqrt(jnp.mean(attended * attended, axis=-1, keepdims=True) + 1e-05)
    mixed_out = (mixed_out * sub_gain.astype(jnp.float32) * LAMBDA_SCALE).astype(jnp.bfloat16)
    mixed_out = mixed_out.reshape(row_count, heads_here * 2 * head_dim)
    product = jnp.dot(mixed_out, out_weight, preferred_element_type=jnp.float32).reshape(
        seq_count, prop_count, -1
    )
    output = sent_and_summed(product.astype(jnp.bfloat16), "tp", 2).astype(jnp.bfloat16)
    return (output, key_out, value_out)


def solution(mesh):
    torus = Mesh(
        mesh.devices.reshape(mesh.shape["dp"], 8, 4, mesh.shape["tp"]), ("dp", "kv_0", "kv_1", "tp")
    )
    placed = (
        P("dp", None, KV),
        P(KV),
        P(KV, "tp"),
        P(KV, "tp"),
        P(KV, "tp"),
        P("tp", KV),
        P("tp"),
        P(),
        P("dp", KV, "tp", None, None),
        P("dp", KV, "tp", None),
        P("dp"),
        P("dp"),
        P("dp", None),
    )
    return jax.shard_map(
        per_device,
        mesh=torus,
        in_specs=placed,
        out_specs=(P("dp", None, KV_TP), P("dp", KV, "tp", None, None), P("dp", KV, "tp", None)),
        check_vma=False,
    )
```

profile of v0, /device:TPU:135, one launch (start us, length us, event | category | flops | bytes accessed | tf_op | source)
XLA Modules:
  0.0 422.1 jit_solution(6596932507538783749)
XLA Ops:
  7.2 4.6 %copy.611 = bf16[16,32,8,2,128]{4,3,2,1,0:T(2,128)(2,1)} copy(bf16[16,32,8,2,128]{4,3,2,1,0:T(2,128)(2,1)} %param.23) | data formatting | bytes 4194304
  14.1 9.4 %all-to-all-start.1 = ((f32[32,1,256]{2,1,0:T(1,128)}), f32[32,1,256]{2,1,0:T(1,128)S(1)}, u32[]{:S(2)}, u32[]{:S(2)}) async-start(f32[32,1,256]{2,1,0:T(1,128)} %reshape.538), calls=%async_computation.1 | async-start | bytes 65536 | tf_op jit(solution)/shard_map/all_to_all | solution.py:20
  25.2 2.8 all-to-all-done.1
  27.9 8.2 %all-to-all-start = ((bf16[128,32,64]{0,2,1:T(8,128)(2,1)}), bf16[128,32,64]{0,2,1:T(8,128)(2,1)S(1)}, u32[]{:S(2)}, u32[]{:S(2)}) async-start(bf16[128,32,64]{0,2,1:T(8,128)(2,1)} %bitcast.3), calls=%async_computation | async-start | bytes 1048576 | tf_op jit(solution)/shard_map/all_to_all | solution.py:159
  36.2 13.2 %all_gather.21 = bf16[256,512]{1,0:T(8,128)(2,1)} all-gather(bf16[256,128]{1,0:T(8,128)(2,1)S(1)} %bitcast.359), channel_id=1, replica_groups=mesh['dp'=4,'kv_0'=8,'kv_1'=4,'tp'=2] {'kv_1'}, dimensions={1}, use_global_device_ids=true | all-gather | bytes 327680 | tf_op jit(solution)/shard_map/all_gather | solution.py:31
  51.1 8.7 %all-to-all-start.2 = ((bf16[128,32,64]{0,2,1:T(8,128)(2,1)}), bf16[128,32,64]{0,2,1:T(8,128)(2,1)}, u32[]{:S(2)}, u32[]{:S(2)}) async-start(bf16[128,32,64]{0,2,1:T(8,128)(2,1)} %bitcast.8), calls=%async_computation.2 | async-start | bytes 1048576 | tf_op jit(solution)/shard_map/all_to_all | solution.py:160
  59.8 5.8 %while.11 = (s32[]{:T(128)}, f32[16,16,16]{2,1,0:T(8,128)S(1)}, s32[16,16]{1,0:T(8,128)S(1)}, s32[]{:T(128)}) while((s32[]{:T(128)}, f32[16,16,16]{2,1,0:T(8,128)S(1)}, s32[16,16]{1,0:T(8,128)S(1)}, s32[]{:T(128)}) %tuple.80), condition=%wide.region_3.0_spmd.clone, body=%wide.region_2.0_spmd.clone.sunk | while | flops 799234 | bytes 68661 | solution.py:106
  68.4 26.0 %all-gather.5.cloned.1.call-done = bf16[256,4096]{1,0:T(8,128)(2,1)} async-done(((bf16[256,512]{1,0:T(8,128)(2,1)}), bf16[256,4096]{1,0:T(8,128)(2,1)}) %all-gather.5.cloned.1.call-update) | async-done | bytes 2097168 | tf_op jit(solution)/shard_map/all_gather | solution.py:31
  94.4 2.5 convolution_multiply_fusion.2
  97.0 8.6 %all-to-all-start.3 = ((bf16[128,32,64]{0,2,1:T(8,128)(2,1)}), bf16[128,32,64]{0,2,1:T(8,128)(2,1)S(1)}, u32[]{:S(2)}, u32[]{:S(2)}) async-start(bf16[128,32,64]{0,2,1:T(8,128)(2,1)} %bitcast.333), calls=%async_computation.3 | async-start | bytes 1048576 | tf_op jit(solution)/shard_map/all_to_all | solution.py:161
  105.7 1.8 convolution_multiply_fusion.1
  108.0 7.6 %all-to-all-done.3 = bf16[128,32,64]{0,2,1:T(8,128)(2,1)S(1)} async-done(((bf16[128,32,64]{0,2,1:T(8,128)(2,1)}), bf16[128,32,64]{0,2,1:T(8,128)(2,1)S(1)}, u32[]{:S(2)}, u32[]{:S(2)}) %all-to-all-start.3) | async-done | bytes 524320 | tf_op jit(solution)/shard_map/all_to_all | solution.py:161
  117.3 77.0 %all-gather.7.cloned.1.call-done = bf16[2048,768]{1,0:T(8,128)(2,1)} async-done(((bf16[64,768]{1,0:T(8,128)(2,1)}), bf16[2048,768]{1,0:T(8,128)(2,1)}) %all-gather.7.cloned.1.call-update) | async-done | bytes 3145744 | tf_op jit(solution)/shard_map/all_gather | solution.py:39
  194.3 3.7 fusion.103
  199.2 4.9 %copy.326 = bf16[256,16,64,2]{2,3,0,1:T(2,128)(2,1)S(1)} copy(bf16[256,16,64,2]{0,3,2,1:T(2,128)(2,1)} %reshape.515) | data formatting | bytes 2097152 | tf_op jit(solution)/shard_map/reshape | solution.py:197
  204.2 1.8 reshape_reshape.4
  205.9 3.3 fusion.110
  212.2 19.2 %all-gather = f32[4096,16]{0,1:T(8,128)S(1)} all-gather(f32[512,16]{0,1:T(8,128)S(1)} %pad_maximum_fusion.3), channel_id=2, replica_groups=mesh['dp'=4,'kv_0'=8,'kv_1'=4,'tp'=2] {'kv_0'}, dimensions={0}, use_global_device_ids=true | all-gather | bytes 294912 | tf_op jit(solution)/shard_map/all_gather | solution.py:57
  231.9 9.4 %all-gather.1 = f32[2048,16]{0,1:T(8,128)S(1)} all-gather(f32[512,16]{0,1:T(8,128)S(1)} %pad_maximum_fusion.4), channel_id=3, replica_groups=mesh['dp'=4,'kv_0'=8,'kv_1'=4,'tp'=2] {'kv_1'}, dimensions={0}, use_global_device_ids=true | all-gather | bytes 163840 | tf_op jit(solution)/shard_map/all_gather | solution.py:57
  244.9 3.9 copy.353
  248.7 4.9 %reshape_reshape.5 = bf16[16,16,8,2,128]{4,1,0,3,2:T(8,128)(2,1)} reshape(bf16[256,16,2,64]{3,2,0,1:T(2,128)(2,1)} %copy.353) | data formatting | bytes 2097152 | tf_op jit(solution)/shard_map/reshape;reshape | solution.py:205
  253.6 2.0 fusion.109
  261.4 80.9 %all-reduce.3.cloned.1.call-done = bf16[16,16,8,256]{3,1,2,0:T(8,128)(2,1)} async-done(((bf16[16,16,8,256]{3,1,2,0:T(8,128)(2,1)}), bf16[16,16,8,256]{3,1,2,0:T(8,128)(2,1)}) %all-reduce.3.cloned.1.call-update) | async-done | bytes 1048592 | tf_op jit(solution)/shard_map/psum | solution.py:77
  342.5 2.3 copy.362
  344.8 2.5 copy.399
  347.3 3.7 copy.368
  351.0 2.6 copy.369
  353.6 29.8 %scatter_fusion = bf16[16,32,8,2,128]{4,3,2,1,0:T(2,128)(2,1)} fusion(bf16[16,32,8,2,128]{4,3,2,1,0:T(2,128)(2,1)} %copy.611, s32[256]{0:T(256)S(1)} %reshape.521, bf16[256,8,2,128]{3,2,1,0:T(2,128)(2,1)} %copy.368), kind=kCustom, calls=%fused_computation | custom fusion | bytes 3147776 | tf_op jit(solution)/shard_map/scatter | solution.py:211
  383.4 14.4 %scatter_fusion.1 = bf16[16,32,8,256]{3,2,1,0:T(8,128)(2,1)S(1)} fusion(bf16[16,32,8,256]{3,2,1,0:T(8,128)(2,1)S(1)} %copy-done.2, s32[256]{0:T(256)S(1)} %reshape.521, bf16[256,8,256]{2,1,0:T(8,128)(2,1)} %copy.369), kind=kCustom, calls=%fused_computation.1 | custom fusion | bytes 3147776 | tf_op jit(solution)/shard_map/scatter | solution.py:212
  397.8 4.3 %select_divide_fusion = f32[16,8,2,16,16]{3,4,2,1,0:T(8,128)} fusion(f32[16,8,2,16,16]{3,4,2,1,0:T(8,128)} %copy-done.7, f32[16,8,2,16]{3,2,1,0:T(2,128)S(1)} %bitcast.337, f32[16,8,2,16]{3,2,1,0:T(2,128)S(1)} %bitcast.339, pred[16,16,16]{1,2,0:T(8,128)(4,1)S(1)} %copy-done.18), kind=kLoop, calls=%fused_computation.17 | loop fusion | flops 196608 | bytes 561152 | tf_op jit(solution)/shard_map/div | solution.py:244
  402.1 2.9 multiply_reduce_fusion
  406.3 8.5 %all_to_all.67 = bf16[2,2,8192]{2,1,0:T(2,128)(2,1)S(1)} all-to-all(bf16[2,2,8192]{2,1,0:T(2,128)(2,1)S(1)} %reshape.540), channel_id=1, replica_groups=mesh['dp'=4,'kv_0'=8,'kv_1'=4,'tp'=2] {'tp'}, dimensions={0} | all-to-all | bytes 131072 | tf_op jit(solution)/shard_map/all_to_all | solution.py:89
  (188 shorter events, 31.9 us)
Async XLA Ops:
  7.2 398.4 %copy-start = (bf16[2048,128]{1,0:T(8,128)(2,1)S(1)}, bf16[2048,128]{1,0:T(8,128)(2,1)}, u32[]{:S(2)}) copy-start(bf16[2048,128]{1,0:T(8,128)(2,1)} %param.20) | copy-start | bytes 1572868
  7.2 4.6 %copy-start.9 = (bf16[16,32,8,256]{3,2,1,0:T(8,128)(2,1)S(1)}, bf16[16,32,8,256]{3,2,1,0:T(8,128)(2,1)}, u32[]{:S(2)}) copy-start(bf16[16,32,8,256]{3,2,1,0:T(8,128)(2,1)} %param.24) | copy-start | bytes 6291460
  11.8 1.4 copy-start.22
  11.8 1.4 copy-start.20
  11.8 11.7 %copy-start.11 = (bf16[128,2048]{1,0:T(8,128)(2,1)S(1)}, bf16[128,2048]{1,0:T(8,128)(2,1)}, u32[]{:S(2)}) copy-start(bf16[128,2048]{1,0:T(8,128)(2,1)} %param.17) | copy-start | bytes 1572868
  13.3 36.1 %copy-start.12 = (bf16[128,2048]{1,0:T(8,128)(2,1)S(1)}, bf16[128,2048]{1,0:T(8,128)(2,1)}, u32[]{:S(2)}) copy-start(bf16[128,2048]{1,0:T(8,128)(2,1)} %param.18) | copy-start | bytes 1572868
  14.1 13.8 %all-to-all-start.1 = ((f32[32,1,256]{2,1,0:T(1,128)}), f32[32,1,256]{2,1,0:T(1,128)S(1)}, u32[]{:S(2)}, u32[]{:S(2)}) async-start(f32[32,1,256]{2,1,0:T(1,128)} %reshape.538), calls=%async_computation.1 | async-start | bytes 65536 | tf_op jit(solution)/shard_map/all_to_all | solution.py:20
  27.9 23.2 %all-to-all-start = ((bf16[128,32,64]{0,2,1:T(8,128)(2,1)}), bf16[128,32,64]{0,2,1:T(8,128)(2,1)S(1)}, u32[]{:S(2)}, u32[]{:S(2)}) async-start(bf16[128,32,64]{0,2,1:T(8,128)(2,1)} %bitcast.3), calls=%async_computation | async-start | bytes 1048576 | tf_op jit(solution)/shard_map/all_to_all | solution.py:159
  36.1 23.7 %copy-start.19 = (s32[16,16]{1,0:T(8,128)S(1)}, s32[16,16]{1,0:T(8,128)}, u32[]{:S(2)}) copy-start(s32[16,16]{1,0:T(8,128)} %param.27) | copy-start | bytes 3076
  36.1 58.3 %all-gather.5.cloned.1.call-start = ((), (), s32[]{:S(2)}) async-start(), calls=%async_computation.5 | async-start | bytes 2359296 | tf_op jit(solution)/shard_map/all_gather | solution.py:31
  51.1 14.5 %copy-start.23 = (s32[16]{0:T(128)S(1)}, s32[16]{0:T(128)}, u32[]{:S(2)}) copy-start(s32[16]{0:T(128)} %param.25) | copy-start | bytes 196
  51.1 14.5 %copy-start.24 = (s32[16]{0:T(128)S(1)}, s32[16]{0:T(128)}, u32[]{:S(2)}) copy-start(s32[16]{0:T(128)} %param.26) | copy-start | bytes 196
  51.1 14.8 %copy-start.13 = (bf16[128,2048]{1,0:T(8,128)(2,1)S(1)}, bf16[128,2048]{1,0:T(8,128)(2,1)}, u32[]{:S(2)}) copy-start(bf16[128,2048]{1,0:T(8,128)(2,1)} %param.19) | copy-start | bytes 1572868
  51.1 45.9 %all-to-all-start.2 = ((bf16[128,32,64]{0,2,1:T(8,128)(2,1)}), bf16[128,32,64]{0,2,1:T(8,128)(2,1)}, u32[]{:S(2)}, u32[]{:S(2)}) async-start(bf16[128,32,64]{0,2,1:T(8,128)(2,1)} %bitcast.8), calls=%async_computation.2 | async-start | bytes 1048576 | tf_op jit(solution)/shard_map/all_to_all | solution.py:160
  94.4 11.2 %copy-start.1 = (bf16[256,4096]{1,0:T(8,128)(2,1)S(1)}, bf16[256,4096]{1,0:T(8,128)(2,1)}, u32[]{:S(2)}) copy-start(bf16[256,4096]{1,0:T(8,128)(2,1)} %all-gather.5.cloned.1.call-done) | copy-start | bytes 6291460
  97.0 18.6 %all-to-all-start.3 = ((bf16[128,32,64]{0,2,1:T(8,128)(2,1)}), bf16[128,32,64]{0,2,1:T(8,128)(2,1)S(1)}, u32[]{:S(2)}, u32[]{:S(2)}) async-start(bf16[128,32,64]{0,2,1:T(8,128)(2,1)} %bitcast.333), calls=%async_computation.3 | async-start | bytes 1048576 | tf_op jit(solution)/shard_map/all_to_all | solution.py:161
  105.6 88.7 %all-gather.7.cloned.1.call-start = ((), (), s32[]{:S(2)}) async-start(), calls=%async_computation.6 | async-start | bytes 3244032 | tf_op jit(solution)/shard_map/all_gather | solution.py:39
  117.0 225.3 %all-reduce.3.cloned.1.call-start = ((), (), s32[]{:S(2)}) async-start(), calls=%async_computation.7 | async-start | bytes 2097152 | tf_op jit(solution)/shard_map/psum | solution.py:77
  117.2 138.4 %copy-start.17 = (pred[16,16,16]{1,2,0:T(8,128)(4,1)}, pred[16,16,16]{1,2,0:T(8,128)(4,1)S(1)}, u32[]{:S(2)}) copy-start(pred[16,16,16]{1,2,0:T(8,128)(4,1)S(1)} %copy.351) | copy-start | bytes 12292
  209.2 1.4 copy-start.5
  212.0 32.2 %copy-start.8 = (bf16[256,2048]{0,1:T(8,128)(2,1)S(1)}, bf16[256,2048]{0,1:T(8,128)(2,1)}, u32[]{:S(2)}) copy-start(bf16[256,2048]{0,1:T(8,128)(2,1)} %get-tuple-element.49) | copy-start | bytes 3145732
  244.9 8.7 %copy-start.4 = (bf16[256,16,64,2]{0,2,3,1:T(8,128)(2,1)}, bf16[256,16,64,2]{0,2,3,1:T(8,128)(2,1)S(1)}, u32[]{:S(2)}) copy-start(bf16[256,16,64,2]{0,2,3,1:T(8,128)(2,1)S(1)} %copy.596) | copy-start | bytes 3145732
  248.7 4.9 %copy-start.10 = (bf16[16,16,8,2,128]{4,1,0,3,2:T(8,128)(2,1)S(1)}, bf16[16,16,8,2,128]{4,1,0,3,2:T(8,128)(2,1)}, u32[]{:S(2)}) copy-start(bf16[16,16,8,2,128]{4,1,0,3,2:T(8,128)(2,1)} %reshape_reshape.4) | copy-start | bytes 3145732
  255.6 1.7 copy-start.7
  255.6 1.5 copy-start.16
  255.7 2.5 copy-start.6
  258.2 1.6 copy-start.2
  258.2 1.6 copy-start.21
  261.3 81.0 %copy-start.25 = (bf16[256]{0:T(256)(128)(2,1)S(1)}, bf16[256]{0:T(256)(128)(2,1)}, u32[]{:S(2)}) copy-start(bf16[256]{0:T(256)(128)(2,1)} %param.22) | copy-start | bytes 1540
  261.3 140.8 %all-reduce.5.cloned.1.call-start = ((), (), s32[]{:S(2)}) async-start(), calls=%async_computation.8 | async-start | bytes 2097152 | tf_op jit(solution)/shard_map/psum | solution.py:77
  383.4 14.4 %copy-start.18 = (pred[16,16,16]{1,2,0:T(8,128)(4,1)S(1)}, pred[16,16,16]{1,2,0:T(8,128)(4,1)}, u32[]{:S(2)}) copy-start(pred[16,16,16]{1,2,0:T(8,128)(4,1)} %copy-done.17) | copy-start | bytes 12292
  397.8 4.3 %copy-start.3 = (bf16[16,32,8,256]{3,2,1,0:T(8,128)(2,1)}, bf16[16,32,8,256]{3,2,1,0:T(8,128)(2,1)S(1)}, u32[]{:S(2)}) copy-start(bf16[16,32,8,256]{3,2,1,0:T(8,128)(2,1)S(1)} %scatter_fusion.1) | copy-start | bytes 6291460
  (2 other events, 2.3 us)
Sparse Core Ops, SparseCore 0:
  49.6 44.8 all-gather.4
  117.2 77.1 all-gather.6
  261.5 80.8 all-reduce.2
  344.5 55.0 all-reduce.4
where the time goes:
time: 429 us; the launch traced here: 422 us
  waiting for transfers between devices  194 us (45%)
  local copies, waits for them, and re-layouts  95.7 us (22%)
  blocking collectives  50.3 us (12%)
  starting transfers between devices  35.1 us (8%)
  matrix products  20.2 us (5%)
  between operations  14.4 us (3%)
  other arithmetic  11.6 us (3%)
    psum x2, waiting for transfers between devices, by_axis(): value = lax.psum(value, axis)  80.9 us
    all_gather x1, waiting for transfers between devices, rows_first(): filled = lax.all_gather(both, axis, axis=0, tiled=True)  77 us
    scatter x1, local copies, waits for them, and re-layouts, per_device(): key_out = key_cache.at[seq_index, slot_index].set(key_blocks, mode='drop')  29.8 us
    all_gather x2, blocking collectives, all_in_one(): both, at, found = (lax.all_gather(jnp.concatenate(lines), axis), 0, {})  28.6 us
    all_gather x1, waiting for transfers between devices, gather_axes(): value = lax.all_gather(value, axis, axis=dim, tiled=True)  26 us
    scatter x1, local copies, waits for them, and re-layouts, per_device(): value_cache.at[seq_index, slot_index].set(value_blocks, mode='drop')  14.4 us
    unnamed x63, local copies, waits for them, and re-layouts  14.4 us
    all_gather x1, blocking collectives, gather_axes(): value = lax.all_gather(value, axis, axis=dim, tiled=True)  13.2 us
  transfers between devices with their start and end apart: 8, of which 5 were waited for; matrix products, arithmetic and copies ran while one was open for 18% of the time, Pallas kernels for 0%

commit v1 on v0

v1 whole, which is shorter than its diff:
```python
import functools
import math

import jax
import jax.numpy as jnp
from jax import lax
from jax.experimental import pallas as pl
from jax.experimental.pallas import tpu as pltpu
from jax.sharding import Mesh
from jax.sharding import PartitionSpec as P

D = 4096
NZ, NY = 8, 4
KV = ("kv_0", "kv_1")
KV_TP = ("kv_0", "kv_1", "tp")
LAMBDA_SCALE = 0.2 + 0.6 * math.exp(-0.6)
NEG_FILL = -1e30
ROOT = 128 ** (-0.5)
F32, BF16 = jnp.float32, jnp.bfloat16
MESH_ID = pl.DeviceIdType.MESH
DMA = pltpu.SemaphoreType.DMA
Z_STEPS = (1, 7, 2, 6, 3, 5, 4)
Y_STEPS = (1, 3, 2)


def places():
    return lax.axis_index("kv_0"), lax.axis_index("kv_1"), lax.axis_index("tp")


def remote(src, dst, send_sem, recv_sem, **where):
    return pltpu.make_async_remote_copy(
        src_ref=src, dst_ref=dst, send_sem=send_sem, recv_sem=recv_sem,
        device_id=where, device_id_type=MESH_ID,
    )


def greet(z, y, c, with_tp):
    barrier = pltpu.get_barrier_semaphore()
    for d in range(1, NZ):
        pl.semaphore_signal(barrier, inc=1, device_id={"kv_0": (z + d) % NZ}, device_id_type=MESH_ID)
    for d in range(1, NY):
        pl.semaphore_signal(barrier, inc=1, device_id={"kv_1": (y + d) % NY}, device_id_type=MESH_ID)
    if with_tp:
        pl.semaphore_signal(barrier, inc=1, device_id={"tp": 1 - c}, device_id_type=MESH_ID)
    pl.semaphore_wait(barrier, NZ - 1 + NY - 1 + int(with_tp))


def gather_2d(buf, z, y, zs, zr, ys, yr):
    def z_copy(d):
        return remote(buf.at[z, y], buf.at[z, y], zs.at[d], zr.at[d], kv_0=(z + d) % NZ)

    def y_copy(k, e):
        row = (z + NZ - k) % NZ
        return remote(buf.at[row, y], buf.at[row, y], ys.at[k, e], yr.at[k, e], kv_1=(y + e) % NY)

    for d in Z_STEPS:
        z_copy(d).start()
    for e in Y_STEPS:
        y_copy(0, e).start()
    for d in Z_STEPS:
        z_copy(d).wait_recv()
        for e in Y_STEPS:
            y_copy(d, e).start()
    for d in Z_STEPS:
        z_copy(d).wait_send()
    for k in (0, *Z_STEPS):
        for e in Y_STEPS:
            y_copy(k, e).wait()


def project_kernel(tok, gain, wq, wk, wv, cs, sn, qg, kvb, tokg, gaing, wbuf, nrm, pq, pkv, zq, zkv,
                   ws, wr, ts, tr, gs, gr, ls, qs, qr, ks, kr, azs, azr, ays, ayr):
    z, y, c = places()
    gaing[y] = jnp.broadcast_to(gain[...], (16, 128))
    greet(z, y, c, False)
    ws_in = (wq, wk, wv)

    def tok_copy(e):
        return remote(tok, tokg.at[y], ts.at[e], tr.at[e], kv_1=(y + e) % NY)

    def gain_copy(e):
        return remote(gaing.at[y], gaing.at[y], gs.at[e], gr.at[e], kv_1=(y + e) % NY)

    def w_copy(m, e):
        to = (y + e) % NY
        cols = pl.ds(pl.multiple_of(to * 512, 512), 512)
        return remote(ws_in[m].at[:, cols], wbuf.at[m, y], ws.at[m, e], wr.at[m, e], kv_1=to)

    for e in Y_STEPS:
        gain_copy(e).start()
        tok_copy(e).start()
    for m in range(3):
        for e in Y_STEPS:
            w_copy(m, e).start()
    mine = pl.ds(pl.multiple_of(y * 512, 512), 512)
    own = [pltpu.make_async_copy(ws_in[m].at[:, mine], wbuf.at[m, y], ls.at[m]) for m in range(3)]
    for o in own:
        o.start()
    tokg[y] = tok[...]
    for e in Y_STEPS:
        gain_copy(e).wait_recv()
        tok_copy(e).wait_recv()
    power = jnp.zeros((256, 1), F32)
    for a in range(NY):
        wide = tokg[a].astype(F32)
        power += jnp.sum(wide * wide, axis=-1, keepdims=True)
        nrm[:, a * 128:(a + 1) * 128] = (wide * gaing[a, 0:1].astype(F32)).astype(BF16)
    high = power.astype(BF16)
    rest = power - high.astype(F32)
    mid = rest.astype(BF16)
    low = (rest - mid.astype(F32)).astype(BF16)
    lane = lax.broadcasted_iota(jnp.int32, (256, 128), 1)
    terms = jnp.where(lane == 0, high.astype(F32), jnp.where(lane == 1, mid.astype(F32), low.astype(F32)))
    terms = jnp.where(lane < 3, terms, 0.0)
    pq[:, :, 512:640] = terms.astype(BF16).reshape(NZ, 32, 128)

    def product(m):
        own[m].wait()
        for e in Y_STEPS:
            w_copy(m, e).wait_recv()
        out = jnp.zeros((256, 512), F32)
        for a in range(NY):
            out += jnp.dot(nrm[:, a * 128:(a + 1) * 128], wbuf[m, a], preferred_element_type=F32)
        return out.astype(BF16).reshape(NZ, 32, 512)

    def q_copy(d):
        to = (z + d) % NZ
        return remote(pq.at[to], zq.at[d], qs.at[d], qr.at[d], kv_0=to)

    def kv_copy(m, d):
        to = (z + d) % NZ
        return remote(pkv.at[m, to], zkv.at[m, d], ks.at[m, d], kr.at[m, d], kv_0=to)

    pq[:, :, 0:512] = product(0)
    for d in Z_STEPS:
        q_copy(d).start()
    for m in range(2):
        pkv[m] = product(m + 1)
        for d in Z_STEPS:
            kv_copy(m, d).start()

    total = pq[z].astype(F32)
    for d in Z_STEPS:
        q_copy(d).wait_recv()
        total += zq[d].astype(F32)
    power = jnp.sum(total[:, 512:640], axis=-1, keepdims=True)
    scale = lax.rsqrt(power / D + 1e-06)
    cos, sin = cs[...], sn[...]

    def turned(block):
        return block * cos + pltpu.roll(block, 64, 1) * sin

    for v in range(4):
        cols = slice(v * 128, (v + 1) * 128)
        turn = turned(total[:, cols] * scale).astype(BF16)
        qg[z, y, 0, :, cols] = turn[0:16]
        qg[z, y, 1, :, cols] = turn[16:32]
    gather_2d(qg, z, y, azs, azr, ays, ayr)

    for m in range(2):
        total = pkv[m, z].astype(F32)
        for d in Z_STEPS:
            kv_copy(m, d).wait_recv()
            total += zkv[m, d].astype(F32)
        for v in range(4):
            block = total[:, v * 128:(v + 1) * 128] * scale
            if m == 0:
                block = turned(block)
            at = m * 512 + v * 128
            kvb[:, at:at + 128] = block.astype(BF16)
    for e in Y_STEPS:
        gain_copy(e).wait_send()
        tok_copy(e).wait_send()
        for m in range(3):
            w_copy(m, e).wait_send()
    for d in Z_STEPS:
        q_copy(d).wait_send()
        for m in range(2):
            kv_copy(m, d).wait_send()


def vmem(n):
    return [pl.BlockSpec(memory_space=pltpu.VMEM)] * n


def project(tokens, gain, wq, wk, wv, cs, sn):
    return pl.pallas_call(
        project_kernel,
        name="project",
        out_shape=(
            jax.ShapeDtypeStruct((NZ, NY, 2, 16, 512), BF16),
            jax.ShapeDtypeStruct((32, 1024), BF16),
        ),
        in_specs=vmem(7),
        out_specs=tuple(vmem(2)),
        scratch_shapes=[
            pltpu.VMEM((NY, 256, 128), BF16),
            pltpu.VMEM((NY, 16, 128), BF16),
            pltpu.VMEM((3, NY, 128, 512), BF16),
            pltpu.VMEM((256, 512), BF16),
            pltpu.VMEM((NZ, 32, 640), BF16),
            pltpu.VMEM((2, NZ, 32, 512), BF16),
            pltpu.VMEM((NZ, 32, 640), BF16),
            pltpu.VMEM((2, NZ, 32, 512), BF16),
            DMA((3, NY)), DMA((3, NY)), DMA((NY,)), DMA((NY,)), DMA((NY,)), DMA((NY,)), DMA((3,)),
            DMA((NZ,)), DMA((NZ,)), DMA((2, NZ)), DMA((2, NZ)),
            DMA((NZ,)), DMA((NZ,)), DMA((NZ, NY)), DMA((NZ, NY)),
        ],
        compiler_params=pltpu.CompilerParams(collective_id=0, has_side_effects=True),
    )(tokens, gain, wq, wk, wv, cs, sn)


def contract(a, b, dims):
    return lax.dot_general(a, b, (dims, ((), ())), preferred_element_type=F32)


def attend_kernel(meta, q_ref, k_ref, v_ref, kv_ref, om_ref, st_ref, acc_ref, pick):
    b = pl.program_id(0)

    @pl.when(b == 0)
    def _():
        out_row = lax.broadcasted_iota(jnp.int32, (256, 256), 0)
        in_row = lax.broadcasted_iota(jnp.int32, (256, 256), 1)
        source = ((out_row % 128) // 8) * 16 + (out_row % 8) * 2 + out_row // 128
        pick[...] = (source == in_row).astype(F32).astype(BF16)

    limit, mine = meta[0, b], meta[1, b]
    halves = [
        jnp.dot(pick[...], k_ref[0, i * 256:(i + 1) * 256], preferred_element_type=F32).astype(BF16)
        for i in range(2)
    ]
    row = lax.broadcasted_iota(jnp.int32, (256, 128), 0)
    lane = lax.broadcasted_iota(jnp.int32, (256, 128), 1)
    live = ((row % 8) == (lane // 16)) & ((row // 8) < limit)
    live = jnp.concatenate([live.astype(F32), om_ref[0] * mine.astype(F32)], axis=0) > 0.5
    values = jnp.concatenate(
        [v_ref[0], kv_ref[0, :, 512:768], kv_ref[0, :, 768:1024]], axis=0
    )
    for m in range(2):
        keys = jnp.concatenate(
            [halves[i][m * 128:(m + 1) * 128] for i in range(2)]
            + [kv_ref[0, :, (h * 2 + m) * 128:(h * 2 + m + 1) * 128] for h in range(2)], axis=0
        )
        queries = jnp.concatenate(
            [q_ref[0, i, 0, :, (h * 2 + m) * 128:(h * 2 + m + 1) * 128] for i in range(NY) for h in range(2)], axis=0
        )
        s = contract(keys, queries, ((1,), (1,))) * ROOT
        s = jnp.where(live, s, NEG_FILL)
        peak = jnp.max(s, axis=0, keepdims=True)
        e = jnp.where(live, jnp.exp(s - peak), 0.0)
        st_ref[0, 0, m:m + 1] = peak
        st_ref[1, 0, m:m + 1] = jnp.sum(e, axis=0, keepdims=True)
        acc_ref[0, m * 128:(m + 1) * 128] = contract(e.astype(BF16), values, ((0,), (0,))).astype(BF16)


def attend(meta, queries, keys, values, own_kv, own_mask):
    return pl.pallas_call(
        attend_kernel,
        name="attend",
        grid_spec=pltpu.PrefetchScalarGridSpec(
            num_scalar_prefetch=1,
            grid=(16,),
            in_specs=[
                pl.BlockSpec((1, NY, 1, 16, 512), lambda b, meta: (b // 2, 0, b % 2, 0, 0)),
                pl.BlockSpec((1, 512, 128), lambda b, meta: (b, 0, 0)),
                pl.BlockSpec((1, 256, 256), lambda b, meta: (b, 0, 0)),
                pl.BlockSpec((1, 16, 1024), lambda b, meta: (b % 2, 0, 0)),
                pl.BlockSpec((1, 32, 128), lambda b, meta: (b % 2, 0, 0)),
            ],
            out_specs=(
                pl.BlockSpec((2, 1, 2, 128), lambda b, meta: (0, b, 0, 0)),
                pl.BlockSpec((1, 256, 256), lambda b, meta: (b, 0, 0)),
            ),
            scratch_shapes=[pltpu.VMEM((256, 256), BF16)],
        ),
        out_shape=(
            jax.ShapeDtypeStruct((2, 16, 2, 128), F32),
            jax.ShapeDtypeStruct((16, 256, 256), BF16),
        ),
    )(meta, queries, keys, values, own_kv.reshape(2, 16, 1024), own_mask)


def merged(parts):
    peak = functools.reduce(jnp.maximum, [p for p, _ in parts])
    total = sum(t * jnp.exp(p - peak) for p, t in parts)
    return peak, total


def finish_kernel(st, acc, lam, sub, wo, out, yst, ysum, zst, gst, bs, ybuf, zsum, zbuf, mg, prod, got,
                  ss, sr, s2, r2, s3, r3, bss, bsr, zs, zr, azs, azr, ays, ayr, cs, cr):
    z, y, c = places()
    greet(z, y, c, True)

    def st_copy(e):
        return remote(st, yst.at[e], ss.at[e], sr.at[e], kv_1=(y + e) % NY)

    for e in Y_STEPS:
        st_copy(e).start()
    parts = [(st[:, 0], st[:, 1])]
    for e in Y_STEPS:
        st_copy(e).wait_recv()
        parts.append((yst[e, :, 0], yst[e, :, 1]))
    peak, total = merged(parts)
    ysum[:, 0] = peak
    ysum[:, 1] = total

    def st_z(d):
        to = (z + d) % NZ
        return remote(ysum.at[to], zst.at[d], s2.at[d], r2.at[d], kv_0=to)

    for d in Z_STEPS:
        st_z(d).start()
    parts = [(ysum[z, 0], ysum[z, 1])]
    for d in Z_STEPS:
        st_z(d).wait_recv()
        parts.append((zst[d, 0], zst[d, 1]))
    peak, total = merged(parts)
    gst[z, 0] = peak
    gst[z, 1] = 1.0 / total

    def g_copy(d):
        return remote(gst.at[z], gst.at[z], s3.at[d], r3.at[d], kv_0=(z + d) % NZ)

    for d in Z_STEPS:
        g_copy(d).start()
    for d in Z_STEPS:
        g_copy(d).wait_recv()

    row = lax.broadcasted_iota(jnp.int32, (128, 128), 0)
    lane = lax.broadcasted_iota(jnp.int32, (128, 128), 1)
    same = row == lane

    def b_copy(zc, e):
        to = (y + e) % NY
        return remote(bs.at[to, zc], ybuf.at[e, zc], bss.at[zc, e], bsr.at[zc, e], kv_1=to)

    def send_z(d):
        to = (z + d) % NZ
        return remote(zsum.at[to], zbuf.at[d], zs.at[d], zr.at[d], kv_0=to)

    def blocks(d, carry):
        zc = (z + d) % NZ
        ratio = jnp.exp(st[zc, 0] - gst[zc, 0]) * gst[zc, 1]
        for s in range(2):
            first = jnp.where(same, ratio[2 * s:2 * s + 1], 0.0)
            second = jnp.where(same, ratio[2 * s + 1:2 * s + 2] * -lam[...], 0.0)
            mix = jnp.concatenate([first, second], axis=1).astype(BF16)
            block = jnp.dot(mix, acc[zc, s], preferred_element_type=F32).astype(BF16)
            for i in range(NY):
                bs[i, zc, s] = block[i * 32:(i + 1) * 32]
        for e in Y_STEPS:
            b_copy(zc, e).start()
        return carry

    lax.fori_loop(1, NZ + 1, blocks, 0)

    def sums(d, carry):
        zc = (z + d) % NZ
        total = bs[y, zc].astype(F32)
        for e in Y_STEPS:
            b_copy(zc, e).wait_recv()
            total += ybuf[e, zc].astype(F32)
        zsum[zc] = total.astype(BF16)

        @pl.when(d < NZ)
        def _():
            send_z(d).start()

        return carry

    lax.fori_loop(1, NZ + 1, sums, 0)
    total = zsum[z].astype(F32)
    for d in range(1, NZ):
        send_z(d).wait_recv()
        total += zbuf[d].astype(F32)
    norm = total * lax.rsqrt(jnp.mean(total * total, axis=-1, keepdims=True) + 1e-05)
    mg[z, y] = (norm * sub[...] * LAMBDA_SCALE).astype(BF16)
    gather_2d(mg, z, y, azs, azr, ays, ayr)
    product = jnp.zeros((256, 128), F32)
    for h in range(8):
        i, k = h // 2, h % 2
        rows = jnp.concatenate(
            [mg[a, i, s, k * 16:(k + 1) * 16] for a in range(NZ) for s in range(2)], axis=0
        )
        product += jnp.dot(rows, wo[h * 256:(h + 1) * 256], preferred_element_type=F32)
    prod[...] = product.astype(BF16)
    swap = remote(prod, got, cs, cr, tp=1 - c)
    swap.start()
    swap.wait()
    result = (prod[...].astype(F32) + got[...].astype(F32)).astype(BF16)
    out[...] = jnp.where(c == 0, result[:, 0:64].astype(F32), result[:, 64:128].astype(F32)).astype(BF16)

    for e in Y_STEPS:
        st_copy(e).wait_send()
    for d in Z_STEPS:
        st_z(d).wait_send()
        g_copy(d).wait_send()
        send_z(d).wait_send()

    def drain(zc, carry):
        for e in Y_STEPS:
            b_copy(zc, e).wait_send()
        return carry

    lax.fori_loop(0, NZ, drain, 0)


def finish(stats, acc, lam, sub, wo):
    return pl.pallas_call(
        finish_kernel,
        name="finish",
        out_shape=jax.ShapeDtypeStruct((256, 64), BF16),
        in_specs=vmem(5),
        out_specs=vmem(1)[0],
        scratch_shapes=[
            pltpu.VMEM((NY, NZ, 2, 4, 128), F32),
            pltpu.VMEM((NZ, 2, 4, 128), F32),
            pltpu.VMEM((NZ, 2, 4, 128), F32),
            pltpu.VMEM((NZ, 2, 4, 128), F32),
            pltpu.VMEM((NY, NZ, 2, 32, 256), BF16),
            pltpu.VMEM((NY, NZ, 2, 32, 256), BF16),
            pltpu.VMEM((NZ, 2, 32, 256), BF16),
            pltpu.VMEM((NZ, 2, 32, 256), BF16),
            pltpu.VMEM((NZ, NY, 2, 32, 256), BF16),
            pltpu.VMEM((256, 128), BF16),
            pltpu.VMEM((256, 128), BF16),
            DMA((NY,)), DMA((NY,)), DMA((NZ,)), DMA((NZ,)), DMA((NZ,)), DMA((NZ,)),
            DMA((NZ, NY)), DMA((NZ, NY)), DMA((NZ,)), DMA((NZ,)),
            DMA((NZ,)), DMA((NZ,)), DMA((NZ, NY)), DMA((NZ, NY)), DMA, DMA,
        ],
        compiler_params=pltpu.CompilerParams(collective_id=1, has_side_effects=True),
    )(stats, acc, lam, sub, wo)


def spread_kernel(kvb, kvg, zs, zr, ys, yr, ls):
    z, y, c = places()
    greet(z, y, c, False)
    upper = z >= NZ // 2

    def z_copy(d):
        return remote(kvb, kvg.at[z, y], zs.at[d], zr.at[d], kv_0=(z + d) % NZ)

    def z_in(d):
        return (z + NZ - d) % NZ

    def y_copy(k, e):
        row = (z + NZ - k) % NZ
        return remote(kvg.at[row, y], kvg.at[row, y], ys.at[k, e], yr.at[k, e], kv_1=(y + e) % NY)

    for d in Z_STEPS:
        @pl.when((z + d) % NZ >= NZ // 2)
        def _():
            z_copy(d).start()

    @pl.when(upper)
    def _():
        own = pltpu.make_async_copy(kvb, kvg.at[z, y], ls)
        own.start()
        own.wait()
        for e in Y_STEPS:
            y_copy(0, e).start()
        for d in Z_STEPS:
            z_copy(d).wait_recv()
            for e in Y_STEPS:
                y_copy(d, e).start()
        for k in (0, *Z_STEPS):
            for e in Y_STEPS:
                y_copy(k, e).wait()

    for d in Z_STEPS:
        @pl.when((z + d) % NZ >= NZ // 2)
        def _():
            z_copy(d).wait_send()


def spread(kvb):
    return pl.pallas_call(
        spread_kernel,
        name="spread",
        out_shape=jax.ShapeDtypeStruct((NZ, NY, 32, 1024), BF16),
        in_specs=vmem(1),
        out_specs=vmem(1)[0],
        scratch_shapes=[DMA((NZ,)), DMA((NZ,)), DMA((NZ, NY)), DMA((NZ, NY)), DMA],
        compiler_params=pltpu.CompilerParams(collective_id=2, has_side_effects=True),
    )(kvb)


def insert_kernel(slot, k_ref, v_ref, nk_ref, nv_ref, ko_ref, vo_ref, kt, vt):
    at = slot[pl.program_id(0)]
    kt[16:48] = k_ref[0]
    vt[16:48] = v_ref[0]
    kt[pl.ds(at, 16)] = nk_ref[0]
    vt[pl.ds(at, 16)] = nv_ref[0]
    ko_ref[0] = kt[16:48]
    vo_ref[0] = vt[16:48]


def insert(slot, keys, values, new_keys, new_values):
    def spec(*shape):
        return pl.BlockSpec((1, *shape), lambda b, slot: (b, 0, 0, 0))

    return pl.pallas_call(
        insert_kernel,
        name="insert",
        grid_spec=pltpu.PrefetchScalarGridSpec(
            num_scalar_prefetch=1,
            grid=(16,),
            in_specs=[spec(32, 16, 128), spec(32, 8, 256), spec(16, 16, 128), spec(16, 8, 256)],
            out_specs=(spec(32, 16, 128), spec(32, 8, 256)),
            scratch_shapes=[pltpu.VMEM((64, 16, 128), BF16), pltpu.VMEM((64, 8, 256), BF16)],
        ),
        out_shape=(
            jax.ShapeDtypeStruct((16, 32, 16, 128), BF16),
            jax.ShapeDtypeStruct((16, 32, 8, 256), BF16),
        ),
    )(slot, keys, values, new_keys, new_values)


def per_device(tokens, in_gain, query_weight, key_weight, value_weight, out_weight, lambdas, sub_gain,
               key_cache, value_cache, cache_len, accepted, parents):
    z, y = lax.axis_index("kv_0"), lax.axis_index("kv_1")
    starts = cache_len + accepted
    offset = (z * NY + y) * 32

    near = lax.dynamic_slice_in_dim(parents, 2 * z, 2, 0)
    number = jnp.arange(16, dtype=jnp.int32)
    reach = jnp.maximum(
        jnp.eye(16, dtype=F32)[None], (near[:, :, None] == number[None, None, :]).astype(F32)
    )
    for _ in range(4):
        reach = jnp.max(reach[:, :, :, None] * reach[:, None, :, :], axis=2)
    depth = (jnp.sum(reach, axis=-1) - 1.0).astype(jnp.int32)
    position = (lax.dynamic_slice_in_dim(starts, 2 * z, 2, 0)[:, None] + depth).reshape(32)
    frequency = 10000.0 ** (-jnp.arange(64, dtype=F32) / 64)
    angles = position.astype(F32)[:, None] * frequency[None, :]
    cosine, sine = jnp.cos(angles), jnp.sin(angles)
    cs = jnp.concatenate([cosine, cosine], axis=1)
    sn = jnp.concatenate([-sine, sine], axis=1)

    head_row = 2 * y + jnp.arange(32) // 16
    head_lane = jnp.arange(128) // 16
    seen = jnp.tile(reach.transpose(0, 2, 1), (1, 2, 8))
    own_mask = jnp.where(head_row[:, None] == head_lane[None, :], seen, 0.0)
    meta = jnp.stack([starts - offset, (jnp.arange(16) // 2 == z).astype(jnp.int32)])

    queries, own_kv = project(
        tokens.reshape(256, 128), in_gain.reshape(1, 128), query_weight, key_weight, value_weight, cs, sn
    )
    stats, acc = attend(
        meta, queries, key_cache.reshape(16, 512, 128), value_cache.reshape(16, 256, 256), own_kv, own_mask
    )
    lam = jnp.repeat(lambdas, 16)[None, :]
    stats = stats.reshape(2, NZ, 4, 128).transpose(1, 0, 2, 3)
    output = finish(
        stats, acc.reshape(NZ, 2, 256, 256), lam, sub_gain.astype(F32).reshape(1, 256), out_weight
    )
    both = spread(own_kv).reshape(NZ, NY, 2, 16, 1024).transpose(0, 2, 3, 1, 4)
    new_keys = both[..., :512].reshape(16, 16, 16, 128)
    new_values = both[..., 512:].reshape(16, 16, 8, 256)
    slot = jnp.clip(starts - offset + 16, 0, 48)
    key_out, value_out = insert(slot, key_cache.reshape(16, 32, 16, 128), value_cache, new_keys, new_values)
    return output.reshape(16, 16, 64), key_out.reshape(key_cache.shape), value_out


def solution(mesh):
    torus = Mesh(mesh.devices.reshape(mesh.shape["dp"], NZ, NY, mesh.shape["tp"]), ("dp", "kv_0", "kv_1", "tp"))
    placed = (
        P("dp", None, KV), P(KV), P(KV, "tp"), P(KV, "tp"), P(KV, "tp"), P("tp", KV), P("tp"), P(),
        P("dp", KV, "tp", None, None), P("dp", KV, "tp", None), P("dp"), P("dp"), P("dp", None),
    )
    return jax.shard_map(
        per_device, mesh=torus, in_specs=placed,
        out_specs=(P("dp", None, KV_TP), P("dp", KV, "tp", None, None), P("dp", KV, "tp", None)),
        check_vma=False,
    )
```

time: 429 us -> 184 us (0.43)
  waiting for transfers between devices: 194 us -> 0 us
  Pallas kernels: 0 us -> 164 us
  local copies, waits for them, and re-layouts: 95.7 us -> 10.6 us
  blocking collectives: 50.3 us -> 0 us
  starting transfers between devices: 35.1 us -> 0 us
  matrix products: 20.2 us -> 0 us
  between operations: 14.4 us -> 0.77 us
  other arithmetic: 11.6 us -> 5.51 us
    pallas_call x0 -> x5, Pallas kernels: none -> 164 us  [the longest x1 51.3 us: finish(): pl.pallas_call(finish_kernel, name='finish', out_shape=jax.ShapeDtypeStru...]
    all_gather x2 -> x0, waiting for transfers between devices: 103 us -> none  [the longest x1 77 us: rows_first(): filled = lax.all_gather(both, axis, axis=0, tiled=True)]
    psum x2 -> x0, waiting for transfers between devices: 80.9 us -> none  [by_axis(): value = lax.psum(value, axis)]
    scatter x2 -> x0, local copies, waits for them, and re-layouts: 44.2 us -> none  [the longest x1 29.8 us: per_device(): key_out = key_cache.at[seq_index, slot_index].set(key_blocks, mode='drop')]
    all_gather x3 -> x0, blocking collectives: 41.8 us -> none  [the longest x2 28.6 us: all_in_one(): both, at, found = (lax.all_gather(jnp.concatenate(lines), axis), 0, {})]
    all_to_all x4 -> x0, starting transfers between devices: 34.9 us -> none  [the longest x1 9.44 us: sent_to_all(): lax.all_to_all(jnp.broadcast_to(value[None], (size, *value.shape)), axis,...]
    dot_general x24 -> x0, matrix products: 20.2 us -> none  [the longest x16 4.91 us: extend(): jnp.einsum('bij,bjk->bik', parent_links, reached, precision=lax.Precision...]
    unnamed x63 -> x5, local copies, waits for them, and re-layouts: 14.4 us -> 0.64 us
  transfers between devices with their start and end apart: 8 -> 0, of which waited for: 5 -> 0; matrix products, arithmetic and copies ran while one was open for 18% -> 0% of each run, Pallas kernels for 0% -> 0%
where the time goes in v1:
time: 184 us; the launch traced here: 181 us
  Pallas kernels  164 us (89%)
  local copies, waits for them, and re-layouts  10.6 us (6%)
  other arithmetic  5.51 us (3%)
    pallas_call x1, Pallas kernels, finish(): pl.pallas_call(finish_kernel, name='finish', out_shape=jax.ShapeDtypeStru...  51.3 us
    pallas_call x1, Pallas kernels, project(): pl.pallas_call(project_kernel, name='project', out_shape=(jax.ShapeDtypeS...  50 us
    pallas_call x1, Pallas kernels, spread(): pl.pallas_call(spread_kernel, name='spread', out_shape=jax.ShapeDtypeStru...  35.5 us
    pallas_call x1, Pallas kernels, attend(): pl.pallas_call(attend_kernel, name='attend', grid_spec=pltpu.PrefetchScal...  16.1 us
    pallas_call x1, Pallas kernels, insert(): pl.pallas_call(insert_kernel, name='insert', grid_spec=pltpu.PrefetchScal...  11.3 us

profile of v1, /device:TPU:135, one launch (start us, length us, event | category | flops | bytes accessed | tf_op | source)
XLA Modules:
  0.0 181.1 jit_solution(14700639931484890157)
XLA Ops:
  0.6 0.0 copy-start
  0.7 1.2 reshape.188
  2.0 1.3 add_clamp_fusion
  3.2 0.1 dynamic_slice.6
  3.3 0.6 pad_add_fusion.meta
  3.9 0.1 broadcast_compare_fusion
  4.0 0.7 broadcast_in_dim.10
  4.7 0.6 broadcast_in_dim_reshape.3.lam
  5.3 0.1 convert_maximum_fusion
  5.4 0.2 multiply_reduce_fusion.3
  5.6 0.1 multiply_reduce_fusion.2
  5.7 0.1 multiply_reduce_fusion.1
  5.9 0.1 multiply_reduce_fusion
  6.0 0.1 reduce_sum.9
  6.1 0.1 add_convert_fusion
  6.2 0.1 convert_element_type.53
  6.3 0.1 copy.19
  6.3 0.1 fusion.1
  6.5 0.7 pad_maximum_fusion
  7.2 0.1 tile.10
  7.3 0.6 broadcast_select_fusion.om_ref
  8.0 50.0 %project.1 = (bf16[8,4,2,16,512]{4,3,2,1,0:T(8,128)(2,1)}, bf16[32,1024]{1,0:T(8,128)(2,1)}) custom-call(bf16[256,128]{1,0:T(8,128)(2,1)} %bitcast.33, bf16[1,128]{1,0:T(2,128)(2,1)} %bitcast.36, bf16[128,2048]{1,0:T(8,128)(2,1)} %wq.1, bf16[128,2048]{1,0:T(8,128)(2,1)} %wk.1, bf16[128,2048]{1,0:T(8,128)(2,1)} %wv.1, f32[32,128]{1,0:T(8,128)} %get-tuple-element.22.cs, ...), custom_call_target="tpu_custom_call" | custom-call | tf_op jit(solution)/shard_map/project/pallas_call | solution.py:187
  58.0 16.1 %attend.1 = (f32[2,16,2,128]{3,2,1,0:T(2,128)}, bf16[16,256,256]{2,1,0:T(8,128)(2,1)}) custom-call(s32[2,16]{1,0:T(2,128)} %pad_add_fusion.meta, bf16[8,4,2,16,512]{4,3,2,1,0:T(8,128)(2,1)} %get-tuple-element.9.q_ref, bf16[16,512,128]{2,1,0:T(8,128)(2,1)} %bitcast.23, bf16[16,256,256]{2,1,0:T(8,128)(2,1)} %bitcast.25, bf16[2,16,1024]{2,1,0:T(8,128)(2,1)} %bitcast.29, ...), custom_call_target="tpu_custom_call" | custom-call | tf_op jit(solution)/shard_map/attend/pallas_call | solution.py:257
  74.1 1.4 copy.25
  75.5 51.3 %finish.1 = bf16[256,64]{1,0:T(8,128)(2,1)} custom-call(f32[8,2,4,128]{3,2,1,0:T(4,128)} %bitcast.32, bf16[8,2,256,256]{3,2,1,0:T(8,128)(2,1)} %bitcast.28, f32[1,128]{1,0:T(1,128)} %broadcast_in_dim_reshape.3.lam, f32[1,256]{1,0:T(1,128)} %bitcast.35, bf16[2048,128]{1,0:T(8,128)(2,1)} %wo.1), custom_call_target="tpu_custom_call" | custom-call | tf_op jit(solution)/shard_map/finish/pallas_call | solution.py:409
  126.8 35.5 %spread.1 = bf16[8,4,32,1024]{3,2,1,0:T(8,128)(2,1)} custom-call(bf16[32,1024]{1,0:T(8,128)(2,1)} %get-tuple-element.10.kvb), custom_call_target="tpu_custom_call" | custom-call | tf_op jit(solution)/shard_map/spread/pallas_call | solution.py:477
  162.3 3.4 %copy.24 = bf16[8,4,2,16,1024]{4,1,3,2,0:T(4,128)(2,1)S(1)} copy(bf16[8,4,2,16,1024]{4,3,2,1,0:T(8,128)(2,1)} %bitcast.27) | data formatting | bytes 4194304 | tf_op jit(solution)/shard_map/reshape | solution.py:557
  165.7 1.1 fusion.3
  166.8 1.2 reshape.186.nv_ref
  168.0 1.2 reshape.185.nk_ref
  169.2 11.3 %insert.1 = (bf16[16,32,16,128]{3,2,1,0:T(8,128)(2,1)}, bf16[16,32,8,256]{3,2,1,0:T(8,128)(2,1)}) custom-call(s32[16]{0:T(128)} %get-tuple-element.15.slot, bf16[16,32,16,128]{3,2,1,0:T(8,128)(2,1)} %bitcast.24, bf16[16,32,8,256]{3,2,1,0:T(8,128)(2,1)} %v_ref.1, bf16[16,16,16,128]{3,2,1,0:T(8,128)(2,1)} %reshape.185.nk_ref, ...), custom_call_target="tpu_custom_call" | custom-call | tf_op jit(solution)/shard_map/insert/pallas_call | solution.py:502
  180.5 0.6 copy.27
  (11 shorter events, 0.1 us)
Async XLA Ops:
  0.6 1.3 copy-start
  169.2 11.3 %copy-start.1 = (bf16[256,64]{1,0:T(8,128)(2,1)S(1)}, bf16[256,64]{1,0:T(8,128)(2,1)}, u32[]{:S(2)}) copy-start(bf16[256,64]{1,0:T(8,128)(2,1)} %finish.1) | copy-start | bytes 98308

commit v2 on v1

v2 whole, which is shorter than its diff:
```python
import functools
import math

import jax
import jax.numpy as jnp
import numpy as np
from jax import lax
from jax.experimental import pallas as pl
from jax.experimental.pallas import tpu as pltpu
from jax.sharding import Mesh
from jax.sharding import PartitionSpec as P

D = 4096
NZ, NY = 8, 4
KV = ("kv_0", "kv_1")
KV_TP = ("kv_0", "kv_1", "tp")
LAMBDA_SCALE = 0.2 + 0.6 * math.exp(-0.6)
NEG_FILL = -1e30
ROOT = 128 ** (-0.5)
F32, BF16 = jnp.float32, jnp.bfloat16
MESH_ID = pl.DeviceIdType.MESH
DMA = pltpu.SemaphoreType.DMA
Z_STEPS = (1, 7, 2, 6, 3, 5, 4)
Y_STEPS = (1, 3, 2)


def places():
    return lax.axis_index("kv_0"), lax.axis_index("kv_1"), lax.axis_index("tp")


def remote(src, dst, send_sem, recv_sem, **where):
    return pltpu.make_async_remote_copy(
        src_ref=src, dst_ref=dst, send_sem=send_sem, recv_sem=recv_sem,
        device_id=where, device_id_type=MESH_ID,
    )


def greet(z, y, c, with_tp):
    barrier = pltpu.get_barrier_semaphore()
    for d in range(1, NZ):
        pl.semaphore_signal(barrier, inc=1, device_id={"kv_0": (z + d) % NZ}, device_id_type=MESH_ID)
    for d in range(1, NY):
        pl.semaphore_signal(barrier, inc=1, device_id={"kv_1": (y + d) % NY}, device_id_type=MESH_ID)
    if with_tp:
        pl.semaphore_signal(barrier, inc=1, device_id={"tp": 1 - c}, device_id_type=MESH_ID)
    pl.semaphore_wait(barrier, NZ - 1 + NY - 1 + int(with_tp))


def gather_2d(buf, z, y, zs, zr, ys, yr):
    def z_copy(d):
        return remote(buf.at[z, y], buf.at[z, y], zs.at[d], zr.at[d], kv_0=(z + d) % NZ)

    def y_copy(k, e):
        row = (z + NZ - k) % NZ
        return remote(buf.at[row, y], buf.at[row, y], ys.at[k, e - 1], yr.at[k, e - 1], kv_1=(y + e) % NY)

    def start():
        for d in Z_STEPS:
            z_copy(d).start()
        for e in Y_STEPS:
            y_copy(0, e).start()

    def hand_on():
        for d in Z_STEPS:
            z_copy(d).wait_recv()
            for e in Y_STEPS:
                y_copy(d, e).start()

    def end():
        for d in Z_STEPS:
            z_copy(d).wait_send()
        for k in (0, *Z_STEPS):
            for e in Y_STEPS:
                y_copy(k, e).wait()

    return start, hand_on, end


def contract(a, b, dims):
    return lax.dot_general(a, b, (dims, ((), ())), preferred_element_type=F32)


def merged(parts):
    peak = functools.reduce(jnp.maximum, [p for p, _ in parts])
    total = sum(t * jnp.exp(p - peak) for p, t in parts)
    return peak, total


def layer_kernel(length, accepted, lambdas, parents, tok, gain, sub, freq, wq, wk, wv, keys_in, values_in, wo_in,
                 out, kvg,
                 tokg, gaing, wbuf, nrm, pq, pkv, zq, zkv, qg, kvown, kc, vc, wo, code, pscr, st, sx, mst, acc, accx,
                 yst, ysum, zst, gst, bs, ybuf, zsum, zbuf, mg, prod, got,
                 ls, ws, wr, ts, tr, gs, gr, qs, qr, ks, kr, azs, azr, ays, ayr, kzs, kzr, kys, kyr,
                 ss, sr, s2, r2, s3, r3, bss, bsr, zs, zr, xs, xr):
    z, y, c = places()
    loads = [
        pltpu.make_async_copy(src, dst, ls.at[3 + i])
        for i, (src, dst) in enumerate(((keys_in, kc), (values_in, vc), (wo_in, wo)))
    ]
    gaing[y] = jnp.broadcast_to(gain[...], (16, 128))
    greet(z, y, c, True)
    ws_in = (wq, wk, wv)

    def tok_copy(e):
        return remote(tok, tokg.at[y], ts.at[e], tr.at[e], kv_1=(y + e) % NY)

    def gain_copy(e):
        return remote(gaing.at[y], gaing.at[y], gs.at[e], gr.at[e], kv_1=(y + e) % NY)

    def w_copy(m, e):
        to = (y + e) % NY
        cols = pl.ds(pl.multiple_of(to * 512, 512), 512)
        return remote(ws_in[m].at[:, cols], wbuf.at[m, y], ws.at[m, e], wr.at[m, e], kv_1=to)

    for e in Y_STEPS:
        gain_copy(e).start()
        tok_copy(e).start()
    for m in range(3):
        for e in Y_STEPS:
            w_copy(m, e).start()
    mine = pl.ds(pl.multiple_of(y * 512, 512), 512)
    own = [pltpu.make_async_copy(ws_in[m].at[:, mine], wbuf.at[m, y], ls.at[m]) for m in range(3)]
    for o in own:
        o.start()
    for load in loads:
        load.start()
    tokg[y] = tok[...]

    row16 = lax.broadcasted_iota(jnp.int32, (16, 16), 0)
    lane16 = lax.broadcasted_iota(jnp.int32, (16, 16), 1)
    unit = (row16 == lane16).astype(F32)
    spread16 = (lax.broadcasted_iota(jnp.int32, (16, 128), 1) % 16 == lax.broadcasted_iota(jnp.int32, (16, 128), 0)).astype(BF16)
    near = parents[pl.ds(2 * z, 2), :]
    seen, angles = [], []
    for s in range(2):
        reach = jnp.maximum(unit, (near[s:s + 1, :] == row16).astype(F32))
        for _ in range(4):
            half = reach.astype(BF16)
            reach = jnp.minimum(jnp.dot(half, half, preferred_element_type=F32), 1.0)
        half = reach.astype(BF16)
        seen.append(jnp.dot(half, spread16, preferred_element_type=F32))
        depth = contract(half, jnp.ones((16, 128), BF16), ((0,), (0,))) - 1.0
        begin = length[2 * z + s] + accepted[2 * z + s]
        angles.append((begin.astype(F32) + depth) * freq[...])
    angle = jnp.concatenate(angles, axis=0)
    cos = jnp.cos(angle)
    sin = jnp.where(lax.broadcasted_iota(jnp.int32, (32, 128), 1) < 64, -1.0, 1.0) * jnp.sin(angle)
    row = lax.broadcasted_iota(jnp.int32, (512, 128), 0)
    lane = lax.broadcasted_iota(jnp.int32, (512, 128), 1)
    code[...] = jnp.where(((row // 2) % 8) == (lane // 16), row // 16, 4096)

    for e in Y_STEPS:
        gain_copy(e).wait_recv()
        tok_copy(e).wait_recv()
    power = jnp.zeros((256, 1), F32)
    for a in range(NY):
        wide = tokg[a].astype(F32)
        power += jnp.sum(wide * wide, axis=-1, keepdims=True)
        nrm[:, a * 128:(a + 1) * 128] = (wide * gaing[a, 0:1].astype(F32)).astype(BF16)
    high = power.astype(BF16)
    rest = power - high.astype(F32)
    mid = rest.astype(BF16)
    low = (rest - mid.astype(F32)).astype(BF16)
    lane = lax.broadcasted_iota(jnp.int32, (256, 128), 1)
    terms = jnp.where(lane == 0, high.astype(F32), jnp.where(lane == 1, mid.astype(F32), low.astype(F32)))
    terms = jnp.where(lane < 3, terms, 0.0)
    pq[:, :, 512:640] = terms.astype(BF16).reshape(NZ, 32, 128)

    def product(m):
        own[m].wait()
        for e in Y_STEPS:
            w_copy(m, e).wait_recv()
        total = jnp.zeros((256, 512), F32)
        for a in range(NY):
            total += jnp.dot(nrm[:, a * 128:(a + 1) * 128], wbuf[m, a], preferred_element_type=F32)
        return total.astype(BF16).reshape(NZ, 32, 512)

    def q_copy(d):
        to = (z + d) % NZ
        return remote(pq.at[to], zq.at[d], qs.at[d], qr.at[d], kv_0=to)

    def kv_copy(m, d):
        to = (z + d) % NZ
        return remote(pkv.at[m, to], zkv.at[m, d], ks.at[m, d], kr.at[m, d], kv_0=to)

    pq[:, :, 0:512] = product(0)
    for d in Z_STEPS:
        q_copy(d).start()
    pkv[0] = product(1)
    for d in Z_STEPS:
        kv_copy(0, d).start()

    total = pq[z].astype(F32)
    for d in Z_STEPS:
        q_copy(d).wait_recv()
        total += zq[d].astype(F32)
    power = jnp.sum(total[:, 512:640], axis=-1, keepdims=True)
    scale = lax.rsqrt(power / D + 1e-06)

    def turned(block):
        return block * cos + pltpu.roll(block, 64, 1) * sin

    for v in range(4):
        cols = slice(v * 128, (v + 1) * 128)
        turn = turned(total[:, cols] * scale).astype(BF16)
        qg[z, y, 0, :, cols] = turn[0:16]
        qg[z, y, 1, :, cols] = turn[16:32]
    q_start, q_hand_on, q_end = gather_2d(qg, z, y, azs, azr, ays, ayr)
    q_start()
    pkv[1] = product(2)
    for d in Z_STEPS:
        kv_copy(1, d).start()
    q_hand_on()

    for m in range(2):
        total = pkv[m, z].astype(F32)
        for d in Z_STEPS:
            kv_copy(m, d).wait_recv()
            total += zkv[m, d].astype(F32)
        for v in range(4):
            block = total[:, v * 128:(v + 1) * 128] * scale
            if m == 0:
                block = turned(block)
            at = m * 512 + v * 128
            kvown[:, at:at + 128] = block.astype(BF16)

    upper = z >= NZ // 2

    def up_z(d):
        return remote(kvown, kvg.at[z, y], kzs.at[d], kzr.at[d], kv_0=(z + d) % NZ)

    def up_y(k, e):
        at = (z + NZ - k) % NZ
        return remote(kvg.at[at, y], kvg.at[at, y], kys.at[k, e - 1], kyr.at[k, e - 1], kv_1=(y + e) % NY)

    own_up = pltpu.make_async_copy(kvown, kvg.at[z, y], ls.at[6])

    def to_upper(d, act):
        @pl.when((z + d) % NZ >= NZ // 2)
        def _():
            act(up_z(d))

    def hand_up(steps):
        @pl.when(upper)
        def _():
            for k in steps:
                if k == 0:
                    own_up.wait()
                else:
                    up_z(k).wait_recv()
                for e in Y_STEPS:
                    up_y(k, e).start()

    for d in Z_STEPS:
        to_upper(d, lambda copy: copy.start())

    @pl.when(upper)
    def _():
        own_up.start()

    q_end()
    loads[0].wait()
    loads[1].wait()

    def queries_of(zc, s):
        return jnp.concatenate(
            [qg[zc, i, s, :, (h * 2 + m) * 128:(h * 2 + m + 1) * 128] for m in range(2) for i in range(NY) for h in range(2)],
            axis=0,
        )

    odd = lax.broadcasted_iota(jnp.int32, (8, 128), 0) % 2 == 1
    offset = (z * NY + y) * 32

    def attend(zc, carry):
        for s in range(2):
            b = 2 * zc + s
            limit = length[b] + accepted[b] - offset
            both = contract(kc[b], queries_of(zc, s), ((1,), (1,)))
            both = both.reshape(64, 8, 256)
            live = (code[...] < limit).reshape(64, 8, 128)
            score = jnp.where(odd[None], both[:, :, 128:], both[:, :, :128]) * ROOT
            score = jnp.where(live, score, NEG_FILL)
            top = jnp.max(score, axis=0)
            peaks = [jnp.max(jnp.where(odd == bool(m), top, NEG_FILL), axis=0, keepdims=True) for m in range(2)]
            peak = jnp.where(odd, peaks[1], peaks[0])
            grown = jnp.where(live, jnp.exp(score - peak[None]), 0.0)
            part = jnp.sum(grown, axis=0)
            for m in range(2):
                st[0, zc, 2 * s + m:2 * s + m + 1] = peaks[m]
                st[1, zc, 2 * s + m:2 * s + m + 1] = jnp.sum(jnp.where(odd == bool(m), part, 0.0), axis=0, keepdims=True)
            pscr[s] = grown.reshape(512, 128)
            chance = jnp.concatenate([pscr[s, pl.ds(m, 256, stride=2), :] for m in range(2)], axis=1).astype(BF16)
            acc[zc, s] = contract(chance, vc[b], ((0,), (0,))).astype(BF16)
        return carry

    lax.fori_loop(0, NZ, attend, 0)

    head_row = 2 * y + lax.broadcasted_iota(jnp.int32, (32, 128), 0) // 16
    head_lane = lax.broadcasted_iota(jnp.int32, (32, 128), 1) // 16
    for s in range(2):
        rows = slice(s * 16, (s + 1) * 16)
        keys = jnp.concatenate(
            [kvown[rows, (h * 2 + m) * 128:(h * 2 + m + 1) * 128] for m in range(2) for h in range(2)], axis=0
        )
        values = jnp.concatenate([kvown[rows, 512:768], kvown[rows, 768:1024]], axis=0)
        both = contract(keys, queries_of(z, s), ((1,), (1,)))
        live = (head_row == head_lane) & (jnp.concatenate([seen[s], seen[s]], axis=0) > 0.5)
        chance = []
        for m in range(2):
            score = jnp.where(live, both[m * 32:(m + 1) * 32, m * 128:(m + 1) * 128] * ROOT, NEG_FILL)
            peak = jnp.max(score, axis=0, keepdims=True)
            grown = jnp.where(live, jnp.exp(score - peak), 0.0)
            sx[0, 2 * s + m:2 * s + m + 1] = peak
            sx[1, 2 * s + m:2 * s + m + 1] = jnp.sum(grown, axis=0, keepdims=True)
            chance.append(grown)
        accx[s] = contract(jnp.concatenate(chance, axis=1).astype(BF16), values, ((0,), (0,))).astype(BF16)
    mst[...] = st[...]
    peak, total = merged([(st[0, z], st[1, z]), (sx[0], sx[1])])
    mst[0, z] = peak
    mst[1, z] = total

    def st_copy(e):
        return remote(mst, yst.at[e], ss.at[e], sr.at[e], kv_1=(y + e) % NY)

    for e in Y_STEPS:
        st_copy(e).start()
    parts = [(mst[0], mst[1])]
    for e in Y_STEPS:
        st_copy(e).wait_recv()
        parts.append((yst[e, 0], yst[e, 1]))
    peak, total = merged(parts)
    ysum[:, 0] = peak
    ysum[:, 1] = total

    def st_z(d):
        to = (z + d) % NZ
        return remote(ysum.at[to], zst.at[d], s2.at[d], r2.at[d], kv_0=to)

    for d in Z_STEPS:
        st_z(d).start()
    hand_up((0, 1, 7, 2))
    parts = [(ysum[z, 0], ysum[z, 1])]
    for d in Z_STEPS:
        st_z(d).wait_recv()
        parts.append((zst[d, 0], zst[d, 1]))
    peak, total = merged(parts)
    gst[z, 0] = peak
    gst[z, 1] = 1.0 / total

    def g_copy(d):
        return remote(gst.at[z], gst.at[z], s3.at[d], r3.at[d], kv_0=(z + d) % NZ)

    for d in Z_STEPS:
        g_copy(d).start()
    row = lax.broadcasted_iota(jnp.int32, (128, 128), 0)
    lane = lax.broadcasted_iota(jnp.int32, (128, 128), 1)
    same = row == lane
    lane = lax.broadcasted_iota(jnp.int32, (1, 128), 1) // 16
    lam = jnp.zeros((1, 128), F32)
    for h in range(8):
        lam = jnp.where(lane == h, -lambdas[h], lam)
    for d in Z_STEPS:
        g_copy(d).wait_recv()

    def b_copy(zc, e):
        to = (y + e) % NY
        return remote(bs.at[to, zc], ybuf.at[e - 1, zc], bss.at[zc, e - 1], bsr.at[zc, e - 1], kv_1=to)

    def send_z(d):
        to = (z + d) % NZ
        return remote(zsum.at[to], zbuf.at[d], zs.at[d], zr.at[d], kv_0=to)

    def mixing(peaks, zc, s):
        ratio = jnp.exp(peaks - gst[zc, 0]) * gst[zc, 1]
        first = jnp.where(same, ratio[2 * s:2 * s + 1], 0.0)
        second = jnp.where(same, ratio[2 * s + 1:2 * s + 2] * lam, 0.0)
        return jnp.concatenate([first, second], axis=1).astype(BF16)

    def send_blocks(zc, last):
        for s in range(2):
            block = jnp.dot(mixing(st[0, zc], zc, s), acc[zc, s], preferred_element_type=F32)
            if last:
                block += jnp.dot(mixing(sx[0], zc, s), accx[s], preferred_element_type=F32)
            block = block.astype(BF16)
            for i in range(NY):
                bs[i, zc, s] = block[i * 32:(i + 1) * 32]
        for e in Y_STEPS:
            b_copy(zc, e).start()

    def blocks(d, carry):
        send_blocks((z + d) % NZ, False)
        return carry

    lax.fori_loop(1, NZ, blocks, 0)
    send_blocks(z, True)
    hand_up((6, 3, 5, 4))

    def sums(d, carry):
        zc = (z + d) % NZ
        total = bs[y, zc].astype(F32)
        for e in Y_STEPS:
            b_copy(zc, e).wait_recv()
            total += ybuf[e - 1, zc].astype(F32)
        zsum[zc] = total.astype(BF16)

        @pl.when(d < NZ)
        def _():
            send_z(d).start()

        return carry

    lax.fori_loop(1, NZ + 1, sums, 0)
    total = zsum[z].astype(F32)
    for d in range(1, NZ):
        send_z(d).wait_recv()
        total += zbuf[d].astype(F32)
    norm = total * lax.rsqrt(jnp.mean(total * total, axis=-1, keepdims=True) + 1e-05)
    mg[z, y] = (norm * sub[...].astype(F32) * LAMBDA_SCALE).astype(BF16)
    m_start, m_hand_on, m_end = gather_2d(mg, z, y, azs, azr, ays, ayr)
    m_start()
    m_hand_on()
    loads[2].wait()
    m_end()
    result = jnp.zeros((256, 128), F32)
    for h in range(8):
        i, k = h // 2, h % 2
        rows = jnp.concatenate(
            [mg[a, i, s, k * 16:(k + 1) * 16] for a in range(NZ) for s in range(2)], axis=0
        )
        result += jnp.dot(rows, wo[h * 256:(h + 1) * 256], preferred_element_type=F32)
    prod[...] = result.astype(BF16)
    swap = remote(prod, got, xs, xr, tp=1 - c)
    swap.start()
    swap.wait()
    result = prod[...].astype(F32) + got[...].astype(F32)
    out[...] = jnp.where(c == 0, result[:, 0:64], result[:, 64:128]).astype(BF16)

    for e in Y_STEPS:
        gain_copy(e).wait_send()
        tok_copy(e).wait_send()
        st_copy(e).wait_send()
        for m in range(3):
            w_copy(m, e).wait_send()
    for d in Z_STEPS:
        q_copy(d).wait_send()
        for m in range(2):
            kv_copy(m, d).wait_send()
        st_z(d).wait_send()
        g_copy(d).wait_send()
        send_z(d).wait_send()
        to_upper(d, lambda copy: copy.wait_send())

    def drain(zc, carry):
        for e in Y_STEPS:
            b_copy(zc, e).wait_send()
        return carry

    lax.fori_loop(0, NZ, drain, 0)

    @pl.when(upper)
    def _():
        for k in (0, *Z_STEPS):
            for e in Y_STEPS:
                up_y(k, e).wait()


def layer(*operands):
    vmem, smem = pl.BlockSpec(memory_space=pltpu.VMEM), pl.BlockSpec(memory_space=pltpu.SMEM)
    anywhere = pl.BlockSpec(memory_space=pl.ANY)
    y_pair, z_pair = [DMA((NY,))] * 2, [DMA((NZ,))] * 2
    zy_pair = [DMA((NZ, NY - 1))] * 2
    return pl.pallas_call(
        layer_kernel,
        name="layer",
        out_shape=(
            jax.ShapeDtypeStruct((256, 64), BF16),
            jax.ShapeDtypeStruct((NZ, NY, 32, 1024), BF16),
        ),
        in_specs=[smem] * 3 + [vmem] * 8 + [anywhere] * 3,
        out_specs=(vmem, anywhere),
        scratch_shapes=[
            pltpu.VMEM((NY, 256, 128), BF16),
            pltpu.VMEM((NY, 16, 128), BF16),
            pltpu.VMEM((3, NY, 128, 512), BF16),
            pltpu.VMEM((256, 512), BF16),
            pltpu.VMEM((NZ, 32, 640), BF16),
            pltpu.VMEM((2, NZ, 32, 512), BF16),
            pltpu.VMEM((NZ, 32, 640), BF16),
            pltpu.VMEM((2, NZ, 32, 512), BF16),
            pltpu.VMEM((NZ, NY, 2, 16, 512), BF16),
            pltpu.VMEM((32, 1024), BF16),
            pltpu.VMEM((16, 512, 128), BF16),
            pltpu.VMEM((16, 256, 256), BF16),
            pltpu.VMEM((2048, 128), BF16),
            pltpu.VMEM((512, 128), jnp.int32),
            pltpu.VMEM((2, 512, 128), F32),
            pltpu.VMEM((2, NZ, 4, 128), F32),
            pltpu.VMEM((2, 4, 128), F32),
            pltpu.VMEM((2, NZ, 4, 128), F32),
            pltpu.VMEM((NZ, 2, 256, 256), BF16),
            pltpu.VMEM((2, 256, 256), BF16),
            pltpu.VMEM((NY, 2, NZ, 4, 128), F32),
            pltpu.VMEM((NZ, 2, 4, 128), F32),
            pltpu.VMEM((NZ, 2, 4, 128), F32),
            pltpu.VMEM((NZ, 2, 4, 128), F32),
            pltpu.VMEM((NY, NZ, 2, 32, 256), BF16),
            pltpu.VMEM((NY - 1, NZ, 2, 32, 256), BF16),
            pltpu.VMEM((NZ, 2, 32, 256), BF16),
            pltpu.VMEM((NZ, 2, 32, 256), BF16),
            pltpu.VMEM((NZ, NY, 2, 32, 256), BF16),
            pltpu.VMEM((256, 128), BF16),
            pltpu.VMEM((256, 128), BF16),
            DMA((7,)), DMA((3, NY)), DMA((3, NY)), *y_pair, *y_pair,
            *z_pair, DMA((2, NZ)), DMA((2, NZ)),
            *z_pair, *zy_pair, *z_pair, *zy_pair,
            *y_pair, *z_pair, *z_pair, *zy_pair, *z_pair, DMA, DMA,
        ],
        compiler_params=pltpu.CompilerParams(
            collective_id=0, has_side_effects=True, vmem_limit_bytes=56 * 1024 * 1024
        ),
    )(*operands)


def insert_kernel(length, accepted, k_ref, v_ref, new_ref, ko_ref, vo_ref, kn, vn, kt, vt):
    b = pl.program_id(0)
    offset = (lax.axis_index("kv_0") * NY + lax.axis_index("kv_1")) * 32
    at = jnp.clip(length[b] + accepted[b] - offset + 16, 0, 48)
    for i in range(NY):
        for v in range(4):
            kn[pl.ds(i * 4 + v, 16, stride=16), :] = new_ref[0, i, 0, :, v * 128:(v + 1) * 128].astype(F32)
        for v in range(4):
            h, half = v // 2, v % 2
            vn[half, pl.ds(i * 2 + h, 16, stride=8), :] = new_ref[0, i, 0, :, 512 + v * 128:640 + v * 128].astype(F32)
    kt[16:48] = k_ref[0]
    vt[16:48] = v_ref[0]
    kt[pl.ds(at, 16)] = kn[...].reshape(16, 16, 128).astype(BF16)
    for half in range(2):
        vt[pl.ds(at, 16), :, half * 128:(half + 1) * 128] = vn[half].reshape(16, 8, 128).astype(BF16)
    ko_ref[0] = kt[16:48]
    vo_ref[0] = vt[16:48]


def insert(length, accepted, keys, values, new):
    def spec(*shape):
        return pl.BlockSpec((1, *shape), lambda b, *_: (b, 0, 0, 0))

    return pl.pallas_call(
        insert_kernel,
        name="insert",
        grid_spec=pltpu.PrefetchScalarGridSpec(
            num_scalar_prefetch=2,
            grid=(16,),
            in_specs=[
                spec(32, 16, 128), spec(32, 8, 256),
                pl.BlockSpec((1, NY, 1, 16, 1024), lambda b, *_: (b // 2, 0, b % 2, 0, 0)),
            ],
            out_specs=(spec(32, 16, 128), spec(32, 8, 256)),
            scratch_shapes=[
                pltpu.VMEM((256, 128), F32), pltpu.VMEM((2, 128, 128), F32),
                pltpu.VMEM((64, 16, 128), BF16), pltpu.VMEM((64, 8, 256), BF16),
            ],
        ),
        out_shape=(
            jax.ShapeDtypeStruct((16, 32, 16, 128), BF16),
            jax.ShapeDtypeStruct((16, 32, 8, 256), BF16),
        ),
    )(length, accepted, keys, values, new)


def per_device(tokens, in_gain, query_weight, key_weight, value_weight, out_weight, lambdas, sub_gain,
               key_cache, value_cache, cache_len, accepted, parents):
    frequency = np.float32(10000.0) ** (-np.arange(64, dtype=np.float32) / np.float32(64))
    frequency = jnp.asarray(np.concatenate([frequency, frequency])[None, :])
    output, new = layer(
        cache_len, accepted, lambdas, parents, tokens.reshape(256, 128), in_gain.reshape(1, 128),
        sub_gain.reshape(1, 256), frequency, query_weight, key_weight, value_weight,
        key_cache.reshape(16, 512, 128), value_cache.reshape(16, 256, 256), out_weight,
    )
    key_out, value_out = insert(
        cache_len, accepted, key_cache.reshape(16, 32, 16, 128), value_cache, new.reshape(NZ, NY, 2, 16, 1024)
    )
    return output.reshape(16, 16, 64), key_out.reshape(key_cache.shape), value_out


def solution(mesh):
    torus = Mesh(mesh.devices.reshape(mesh.shape["dp"], NZ, NY, mesh.shape["tp"]), ("dp", "kv_0", "kv_1", "tp"))
    placed = (
        P("dp", None, KV), P(KV), P(KV, "tp"), P(KV, "tp"), P(KV, "tp"), P("tp", KV), P("tp"), P(),
        P("dp", KV, "tp", None, None), P("dp", KV, "tp", None), P("dp"), P("dp"), P("dp", None),
    )
    return jax.shard_map(
        per_device, mesh=torus, in_specs=placed,
        out_specs=(P("dp", None, KV_TP), P("dp", KV, "tp", None, None), P("dp", KV, "tp", None)),
        check_vma=False,
    )
```

time: 184 us -> 123 us (0.67); the launches traced: 181 us -> 123 us
  Pallas kernels: 164 us -> 120 us
  local copies, waits for them, and re-layouts: 10.6 us -> 1.85 us
  other arithmetic: 5.51 us -> 0 us
    pallas_call x4 -> x1, Pallas kernels: 153 us -> 108 us  [layer(): pl.pallas_call(layer_kernel, name='layer', out_shape=(jax.ShapeDtypeStruc...]
    reshape x4 -> x1, local copies, waits for them, and re-layouts: 7.14 us -> 1.22 us  [per_device(): sub_gain.reshape(1, 256)]
where the time goes in v2:
time: 123 us
  Pallas kernels  120 us (98%)
  local copies, waits for them, and re-layouts  1.85 us (2%)
    pallas_call x1, Pallas kernels, layer(): pl.pallas_call(layer_kernel, name='layer', out_shape=(jax.ShapeDtypeStruc...  108 us
    pallas_call x1, Pallas kernels, insert(): pl.pallas_call(insert_kernel, name='insert', grid_spec=pltpu.PrefetchScal...  12.2 us

profile of v2, /device:TPU:135, one launch (start us, length us, event | category | flops | bytes accessed | tf_op | source)
XLA Modules:
  0.0 122.6 jit_solution(12338693087825625371)
XLA Ops:
  0.6 1.2 reshape.35.sub
  1.9 108.0 %layer.1 = (bf16[256,64]{1,0:T(8,128)(2,1)}, bf16[8,4,32,1024]{3,2,1,0:T(8,128)(2,1)}) custom-call(s32[16]{0:T(128)} %length.3, s32[16]{0:T(128)} %accepted.3, f32[8]{0:T(128)} %lambdas.1, s32[16,16]{1,0:T(8,128)} %parents.1, bf16[256,128]{1,0:T(8,128)(2,1)} %bitcast.13, bf16[1,128]{1,0:T(2,128)(2,1)} %bitcast.14, bf16[1,256]{1,0:T(2,128)(2,1)} %reshape.35.sub, ...), custom_call_target="tpu_custom_call" | custom-call | tf_op jit(solution)/shard_map/layer/pallas_call | solution.py:472
  109.8 0.0 copy-start
  109.8 12.2 %insert.1 = (bf16[16,32,16,128]{3,2,1,0:T(8,128)(2,1)}, bf16[16,32,8,256]{3,2,1,0:T(8,128)(2,1)}) custom-call(s32[16]{0:T(128)} %length.3, s32[16]{0:T(128)} %accepted.3, bf16[16,32,16,128]{3,2,1,0:T(8,128)(2,1)} %bitcast.9, bf16[16,32,8,256]{3,2,1,0:T(8,128)(2,1)} %v_ref.1, bf16[8,4,2,16,1024]{4,3,2,1,0:T(8,128)(2,1)} %bitcast.11), custom_call_target="tpu_custom_call" | custom-call | tf_op jit(solution)/shard_map/insert/pallas_call | solution.py:547
  122.0 0.0 copy-done
  122.0 0.6 copy.18
Async XLA Ops:
  109.8 12.2 %copy-start = (bf16[256,64]{1,0:T(8,128)(2,1)S(1)}, bf16[256,64]{1,0:T(8,128)(2,1)}, u32[]{:S(2)}) copy-start(bf16[256,64]{1,0:T(8,128)(2,1)} %get-tuple-element.7) | copy-start | bytes 98308

commit v3 on v2

--- a/solution.py
+++ b/solution.py
@@ -60,38 +60,35 @@
         for e in Y_STEPS:
             y_copy(0, e).start()
 
-    def hand_on():
-        for d in Z_STEPS:
-            z_copy(d).wait_recv()
-            for e in Y_STEPS:
-                y_copy(d, e).start()
+    def hand_on(d):
+        z_copy(d).wait_recv()
+        for e in Y_STEPS:
+            y_copy(d, e).start()
+
+    def arrived(k):
+        for e in Y_STEPS:
+            y_copy(k, e).wait_recv()
 
     def end():
         for d in Z_STEPS:
             z_copy(d).wait_send()
         for k in (0, *Z_STEPS):
             for e in Y_STEPS:
-                y_copy(k, e).wait()
-
-    return start, hand_on, end
+                y_copy(k, e).wait_send()
+
+    return start, hand_on, arrived, end
 
 
 def contract(a, b, dims):
     return lax.dot_general(a, b, (dims, ((), ())), preferred_element_type=F32)
 
 
-def merged(parts):
-    peak = functools.reduce(jnp.maximum, [p for p, _ in parts])
-    total = sum(t * jnp.exp(p - peak) for p, t in parts)
-    return peak, total
-
-
 def layer_kernel(length, accepted, lambdas, parents, tok, gain, sub, freq, wq, wk, wv, keys_in, values_in, wo_in,
-                 out, kvg,
-                 tokg, gaing, wbuf, nrm, pq, pkv, zq, zkv, qg, kvown, kc, vc, wo, code, pscr, st, sx, mst, acc, accx,
-                 yst, ysum, zst, gst, bs, ybuf, zsum, zbuf, mg, prod, got,
+                 out, kg, vg,
+                 tokg, gaing, wbuf, nrm, pq0, pq1, pkv, zq0, zq1, zkv, qg, kvown, knew, vnew, turn, kc, vc, wo, code, pscr, st, sx, mst, acc, accx,
+                 yst, zst, gst, bs, ybuf, zsum, zbuf, mg, prod, got,
                  ls, ws, wr, ts, tr, gs, gr, qs, qr, ks, kr, azs, azr, ays, ayr, kzs, kzr, kys, kyr,
-                 ss, sr, s2, r2, s3, r3, bss, bsr, zs, zr, xs, xr):
+                 ss, sr, s2, r2, bss, bsr, zs, zr, xs, xr):
     z, y, c = places()
     loads = [
         pltpu.make_async_copy(src, dst, ls.at[3 + i])
@@ -107,17 +104,21 @@
     def gain_copy(e):
         return remote(gaing.at[y], gaing.at[y], gs.at[e], gr.at[e], kv_1=(y + e) % NY)
 
-    def w_copy(m, e):
+    pieces = ((0, 0, 256), (0, 256, 256), (1, 0, 512), (2, 0, 512))
+
+    def w_copy(i, e):
         to = (y + e) % NY
-        cols = pl.ds(pl.multiple_of(to * 512, 512), 512)
-        return remote(ws_in[m].at[:, cols], wbuf.at[m, y], ws.at[m, e], wr.at[m, e], kv_1=to)
+        m, first, size = pieces[i]
+        cols = pl.ds(pl.multiple_of(to * 512 + first, 256), size)
+        into = wbuf.at[m, y, :, first:first + size]
+        return remote(ws_in[m].at[:, cols], into, ws.at[i, e], wr.at[i, e], kv_1=to)
 
     for e in Y_STEPS:
         gain_copy(e).start()
         tok_copy(e).start()
-    for m in range(3):
-        for e in Y_STEPS:
-            w_copy(m, e).start()
+    for i in range(4):
+        for e in Y_STEPS:
+            w_copy(i, e).start()
     mine = pl.ds(pl.multiple_of(y * 512, 512), 512)
     own = [pltpu.make_async_copy(ws_in[m].at[:, mine], wbuf.at[m, y], ls.at[m]) for m in range(3)]
     for o in own:
@@ -164,37 +165,47 @@
     lane = lax.broadcasted_iota(jnp.int32, (256, 128), 1)
     terms = jnp.where(lane == 0, high.astype(F32), jnp.where(lane == 1, mid.astype(F32), low.astype(F32)))
     terms = jnp.where(lane < 3, terms, 0.0)
-    pq[:, :, 512:640] = terms.astype(BF16).reshape(NZ, 32, 128)
-
-    def product(m):
-        own[m].wait()
-        for e in Y_STEPS:
-            w_copy(m, e).wait_recv()
-        total = jnp.zeros((256, 512), F32)
+    pq0[:, :, 256:384] = terms.astype(BF16).reshape(NZ, 32, 128)
+
+    def product(i):
+        m, first, size = pieces[i]
+        if first == 0:
+            own[m].wait()
+        for e in Y_STEPS:
+            w_copy(i, e).wait_recv()
+        total = jnp.zeros((256, size), F32)
         for a in range(NY):
-            total += jnp.dot(nrm[:, a * 128:(a + 1) * 128], wbuf[m, a], preferred_element_type=F32)
-        return total.astype(BF16).reshape(NZ, 32, 512)
-
-    def q_copy(d):
+            total += jnp.dot(
+                nrm[:, a * 128:(a + 1) * 128], wbuf[m, a, :, first:first + size], preferred_element_type=F32
+            )
+        return total.astype(BF16).reshape(NZ, 32, size)
+
+    halves = ((pq0, zq0), (pq1, zq1))
+
+    def q_copy(i, d):
         to = (z + d) % NZ
-        return remote(pq.at[to], zq.at[d], qs.at[d], qr.at[d], kv_0=to)
+        return remote(halves[i][0].at[to], halves[i][1].at[d], qs.at[i, d], qr.at[i, d], kv_0=to)
 
     def kv_copy(m, d):
         to = (z + d) % NZ
         return remote(pkv.at[m, to], zkv.at[m, d], ks.at[m, d], kr.at[m, d], kv_0=to)
 
-    pq[:, :, 0:512] = product(0)
-    for d in Z_STEPS:
-        q_copy(d).start()
-    pkv[0] = product(1)
-    for d in Z_STEPS:
-        kv_copy(0, d).start()
-
-    total = pq[z].astype(F32)
-    for d in Z_STEPS:
-        q_copy(d).wait_recv()
-        total += zq[d].astype(F32)
-    power = jnp.sum(total[:, 512:640], axis=-1, keepdims=True)
+    pq0[:, :, 0:256] = product(0)
+    for d in Z_STEPS:
+        q_copy(0, d).start()
+    pq1[...] = product(1)
+    for d in Z_STEPS:
+        q_copy(1, d).start()
+    pkv[0] = product(2)
+
+    totals = []
+    for i in range(2):
+        total = halves[i][0][z].astype(F32)
+        for d in Z_STEPS:
+            q_copy(i, d).wait_recv()
+            total += halves[i][1][d].astype(F32)
+        totals.append(total)
+    power = jnp.sum(totals[0][:, 256:384], axis=-1, keepdims=True)
     scale = lax.rsqrt(power / D + 1e-06)
 
     def turned(block):
@@ -202,17 +213,20 @@
 
     for v in range(4):
         cols = slice(v * 128, (v + 1) * 128)
-        turn = turned(total[:, cols] * scale).astype(BF16)
-        qg[z, y, 0, :, cols] = turn[0:16]
-        qg[z, y, 1, :, cols] = turn[16:32]
-    q_start, q_hand_on, q_end = gather_2d(qg, z, y, azs, azr, ays, ayr)
+        block = turned(totals[v // 2][:, v % 2 * 128:v % 2 * 128 + 128] * scale).astype(BF16)
+        qg[z, y, 0, :, cols] = block[0:16]
+        qg[z, y, 1, :, cols] = block[16:32]
+    q_start, q_hand_on, q_arrived, q_end = gather_2d(qg, z, y, azs, azr, ays, ayr)
     q_start()
-    pkv[1] = product(2)
+    for d in Z_STEPS:
+        kv_copy(0, d).start()
+    for d in Z_STEPS:
+        q_hand_on(d)
+    pkv[1] = product(3)
     for d in Z_STEPS:
         kv_copy(1, d).start()
-    q_hand_on()
-
-    for m in range(2):
+
+    def finished(m):
         total = pkv[m, z].astype(F32)
         for d in Z_STEPS:
             kv_copy(m, d).wait_recv()
@@ -223,42 +237,56 @@
                 block = turned(block)
             at = m * 512 + v * 128
             kvown[:, at:at + 128] = block.astype(BF16)
+            turn[m, pl.ds((v % 2) * 2 + v // 2 if m else v, 32, stride=4), :] = block
 
     upper = z >= NZ // 2
 
-    def up_z(d):
-        return remote(kvown, kvg.at[z, y], kzs.at[d], kzr.at[d], kv_0=(z + d) % NZ)
-
-    def up_y(k, e):
-        at = (z + NZ - k) % NZ
-        return remote(kvg.at[at, y], kvg.at[at, y], kys.at[k, e - 1], kyr.at[k, e - 1], kv_1=(y + e) % NY)
-
-    own_up = pltpu.make_async_copy(kvown, kvg.at[z, y], ls.at[6])
-
-    def to_upper(d, act):
-        @pl.when((z + d) % NZ >= NZ // 2)
-        def _():
-            act(up_z(d))
-
-    def hand_up(steps):
+    pairs = ((knew, kg), (vnew, vg))
+
+    def up_z(m, d):
+        return remote(pairs[m][0], pairs[m][1].at[z, y], kzs.at[m, d], kzr.at[m, d], kv_0=(z + d) % NZ)
+
+    def up_y(m, k, e):
+        block = pairs[m][1].at[(z + NZ - k) % NZ, y]
+        return remote(block, block, kys.at[m, k, e - 1], kyr.at[m, k, e - 1], kv_1=(y + e) % NY)
+
+    own_up = [pltpu.make_async_copy(pairs[m][0], pairs[m][1].at[z, y], ls.at[6 + m]) for m in range(2)]
+
+    def relay(m, k):
+        at, to = (z + NZ - k) % NZ, (y + (1, 3)[m]) % NY
+        block = pairs[m][1].at[at, (y + (3, 1)[m]) % NY]
+        return remote(block, block, kys.at[m, k, 1], kyr.at[m, k, 1], kv_1=to)
+
+    def to_upper(m, act):
+        for d in Z_STEPS:
+            @pl.when((z + d) % NZ >= NZ // 2)
+            def _():
+                act(up_z(m, d))
+
+    def go_up(m):
+        to_upper(m, lambda copy: copy.start())
+
         @pl.when(upper)
         def _():
-            for k in steps:
-                if k == 0:
-                    own_up.wait()
-                else:
-                    up_z(k).wait_recv()
-                for e in Y_STEPS:
-                    up_y(k, e).start()
-
-    for d in Z_STEPS:
-        to_upper(d, lambda copy: copy.start())
-
-    @pl.when(upper)
-    def _():
-        own_up.start()
-
-    q_end()
+            own_up[m].start()
+
+    def hand_up(m):
+        @pl.when(upper)
+        def _():
+            own_up[m].wait()
+            for k in (0, *Z_STEPS):
+                if k:
+                    up_z(m, k).wait_recv()
+                for e in (1, 3):
+                    up_y(m, k, e).start()
+
+    def hand_over(m):
+        @pl.when(upper)
+        def _():
+            for k in (0, *Z_STEPS):
+                up_y(m, k, (1, 3)[m]).wait_recv()
+                relay(m, k).start()
+
     loads[0].wait()
     loads[1].wait()
 
@@ -271,7 +299,13 @@
     odd = lax.broadcasted_iota(jnp.int32, (8, 128), 0) % 2 == 1
     offset = (z * NY + y) * 32
 
-    def attend(zc, carry):
+    def nth(step):
+        return jnp.where(step % 2 == 1, (step + 1) // 2, (NZ - step // 2) % NZ)
+
+    def attend(step, carry):
+        k = nth(step)
+        q_arrived(k)
+        zc = (z + NZ - k) % NZ
         for s in range(2):
             b = 2 * zc + s
             limit = length[b] + accepted[b] - offset
@@ -293,7 +327,16 @@
             acc[zc, s] = contract(chance, vc[b], ((0,), (0,))).astype(BF16)
         return carry
 
-    lax.fori_loop(0, NZ, attend, 0)
+    lax.fori_loop(0, NZ - 2, attend, 0)
+    finished(0)
+    knew[...] = turn[0].astype(BF16).reshape(32, 4, 128)
+    go_up(0)
+
+    lax.fori_loop(NZ - 2, NZ, attend, 0)
+    q_end()
+    finished(1)
+    vnew[...] = turn[1].astype(BF16).reshape(32, 2, 2, 128)
+    go_up(1)
 
     head_row = 2 * y + lax.broadcasted_iota(jnp.int32, (32, 128), 0) // 16
     head_lane = lax.broadcasted_iota(jnp.int32, (32, 128), 1) // 16
@@ -314,44 +357,33 @@
             sx[1, 2 * s + m:2 * s + m + 1] = jnp.sum(grown, axis=0, keepdims=True)
             chance.append(grown)
         accx[s] = contract(jnp.concatenate(chance, axis=1).astype(BF16), values, ((0,), (0,))).astype(BF16)
-    mst[...] = st[...]
-    peak, total = merged([(st[0, z], st[1, z]), (sx[0], sx[1])])
-    mst[0, z] = peak
-    mst[1, z] = total
+    def log_sum(peak, total):
+        return peak + jnp.log(jnp.maximum(total, 1e-30))
+
+    def joined(parts):
+        peak = functools.reduce(jnp.maximum, parts)
+        return log_sum(peak, sum(jnp.exp(part - peak) for part in parts))
+
+    mst[...] = log_sum(st[0], st[1])
+    mst[z] = joined([mst[z], log_sum(sx[0], sx[1])])
 
     def st_copy(e):
         return remote(mst, yst.at[e], ss.at[e], sr.at[e], kv_1=(y + e) % NY)
 
     for e in Y_STEPS:
         st_copy(e).start()
-    parts = [(mst[0], mst[1])]
+    parts = [mst[...]]
     for e in Y_STEPS:
         st_copy(e).wait_recv()
-        parts.append((yst[e, 0], yst[e, 1]))
-    peak, total = merged(parts)
-    ysum[:, 0] = peak
-    ysum[:, 1] = total
+        parts.append(yst[e])
+    zst[0] = joined(parts)
 
     def st_z(d):
-        to = (z + d) % NZ
-        return remote(ysum.at[to], zst.at[d], s2.at[d], r2.at[d], kv_0=to)
+        return remote(zst.at[0], zst.at[d], s2.at[d], r2.at[d], kv_0=(z + d) % NZ)
 
     for d in Z_STEPS:
         st_z(d).start()
-    hand_up((0, 1, 7, 2))
-    parts = [(ysum[z, 0], ysum[z, 1])]
-    for d in Z_STEPS:
-        st_z(d).wait_recv()
-        parts.append((zst[d, 0], zst[d, 1]))
-    peak, total = merged(parts)
-    gst[z, 0] = peak
-    gst[z, 1] = 1.0 / total
-
-    def g_copy(d):
-        return remote(gst.at[z], gst.at[z], s3.at[d], r3.at[d], kv_0=(z + d) % NZ)
-
-    for d in Z_STEPS:
-        g_copy(d).start()
+    hand_up(0)
     row = lax.broadcasted_iota(jnp.int32, (128, 128), 0)
     lane = lax.broadcasted_iota(jnp.int32, (128, 128), 1)
     same = row == lane
@@ -360,7 +392,8 @@
     for h in range(8):
         lam = jnp.where(lane == h, -lambdas[h], lam)
     for d in Z_STEPS:
-        g_copy(d).wait_recv()
+        st_z(d).wait_recv()
+    gst[...] = joined([zst[d] for d in range(NZ)])
 
     def b_copy(zc, e):
         to = (y + e) % NY
@@ -371,7 +404,7 @@
         return remote(zsum.at[to], zbuf.at[d], zs.at[d], zr.at[d], kv_0=to)
 
     def mixing(peaks, zc, s):
-        ratio = jnp.exp(peaks - gst[zc, 0]) * gst[zc, 1]
+        ratio = jnp.exp(peaks - gst[zc])
         first = jnp.where(same, ratio[2 * s:2 * s + 1], 0.0)
         second = jnp.where(same, ratio[2 * s + 1:2 * s + 2] * lam, 0.0)
         return jnp.concatenate([first, second], axis=1).astype(BF16)
@@ -393,8 +426,6 @@
 
     lax.fori_loop(1, NZ, blocks, 0)
     send_blocks(z, True)
-    hand_up((6, 3, 5, 4))
-
     def sums(d, carry):
         zc = (z + d) % NZ
         total = bs[y, zc].astype(F32)
@@ -410,17 +441,22 @@
         return carry
 
     lax.fori_loop(1, NZ + 1, sums, 0)
+    hand_up(1)
+    hand_over(0)
     total = zsum[z].astype(F32)
     for d in range(1, NZ):
         send_z(d).wait_recv()
         total += zbuf[d].astype(F32)
     norm = total * lax.rsqrt(jnp.mean(total * total, axis=-1, keepdims=True) + 1e-05)
-    mg[z, y] = (norm * sub[...].astype(F32) * LAMBDA_SCALE).astype(BF16)
-    m_start, m_hand_on, m_end = gather_2d(mg, z, y, azs, azr, ays, ayr)
+    mg[z, y] = (norm * sub[...].astype(F32).reshape(1, 256) * LAMBDA_SCALE).astype(BF16)
+    m_start, m_hand_on, m_arrived, m_end = gather_2d(mg, z, y, azs, azr, ays, ayr)
     m_start()
-    m_hand_on()
+    for d in Z_STEPS:
+        m_hand_on(d)
+    hand_over(1)
     loads[2].wait()
-    m_end()
+    for k in (0, *Z_STEPS):
+        m_arrived(k)
     result = jnp.zeros((256, 128), F32)
     for h in range(8):
         i, k = h // 2, h % 2
@@ -439,16 +475,19 @@
         gain_copy(e).wait_send()
         tok_copy(e).wait_send()
         st_copy(e).wait_send()
-        for m in range(3):
-            w_copy(m, e).wait_send()
-    for d in Z_STEPS:
-        q_copy(d).wait_send()
+        for i in range(4):
+            w_copy(i, e).wait_send()
+    for d in Z_STEPS:
+        for i in range(2):
+            q_copy(i, d).wait_send()
         for m in range(2):
             kv_copy(m, d).wait_send()
         st_z(d).wait_send()
-        g_copy(d).wait_send()
         send_z(d).wait_send()
-        to_upper(d, lambda copy: copy.wait_send())
+
+    m_end()
+    for m in range(2):
+        to_upper(m, lambda copy: copy.wait_send())
 
     def drain(zc, carry):
         for e in Y_STEPS:
@@ -459,14 +498,17 @@
 
     @pl.when(upper)
     def _():
-        for k in (0, *Z_STEPS):
-            for e in Y_STEPS:
-                up_y(k, e).wait()
+        for m in range(2):
+            for k in (0, *Z_STEPS):
+                up_y(m, k, 1).wait_send()
+                up_y(m, k, 3).wait_send()
+                up_y(m, k, (3, 1)[m]).wait_recv()
+                relay(m, k).wait()
 
 
 def layer(*operands):
     vmem, smem = pl.BlockSpec(memory_space=pltpu.VMEM), pl.BlockSpec(memory_space=pltpu.SMEM)
-    anywhere = pl.BlockSpec(memory_space=pl.ANY)
+    anywhere = pl.BlockSpec(memory_space=pltpu.HBM)
     y_pair, z_pair = [DMA((NY,))] * 2, [DMA((NZ,))] * 2
     zy_pair = [DMA((NZ, NY - 1))] * 2
     return pl.pallas_call(
@@ -474,21 +516,27 @@
         name="layer",
         out_shape=(
             jax.ShapeDtypeStruct((256, 64), BF16),
-            jax.ShapeDtypeStruct((NZ, NY, 32, 1024), BF16),
+            jax.ShapeDtypeStruct((NZ, NY, 32, 4, 128), BF16),
+            jax.ShapeDtypeStruct((NZ, NY, 32, 2, 2, 128), BF16),
         ),
         in_specs=[smem] * 3 + [vmem] * 8 + [anywhere] * 3,
-        out_specs=(vmem, anywhere),
+        out_specs=(vmem, anywhere, anywhere),
         scratch_shapes=[
             pltpu.VMEM((NY, 256, 128), BF16),
             pltpu.VMEM((NY, 16, 128), BF16),
             pltpu.VMEM((3, NY, 128, 512), BF16),
             pltpu.VMEM((256, 512), BF16),
-            pltpu.VMEM((NZ, 32, 640), BF16),
+            pltpu.VMEM((NZ, 32, 384), BF16),
+            pltpu.VMEM((NZ, 32, 256), BF16),
             pltpu.VMEM((2, NZ, 32, 512), BF16),
-            pltpu.VMEM((NZ, 32, 640), BF16),
+            pltpu.VMEM((NZ, 32, 384), BF16),
+            pltpu.VMEM((NZ, 32, 256), BF16),
             pltpu.VMEM((2, NZ, 32, 512), BF16),
             pltpu.VMEM((NZ, NY, 2, 16, 512), BF16),
             pltpu.VMEM((32, 1024), BF16),
+            pltpu.VMEM((32, 4, 128), BF16),
+            pltpu.VMEM((32, 2, 2, 128), BF16),
+            pltpu.VMEM((2, 128, 128), F32),
             pltpu.VMEM((16, 512, 128), BF16),
             pltpu.VMEM((16, 256, 256), BF16),
             pltpu.VMEM((2048, 128), BF16),
@@ -496,13 +544,12 @@
             pltpu.VMEM((2, 512, 128), F32),
             pltpu.VMEM((2, NZ, 4, 128), F32),
             pltpu.VMEM((2, 4, 128), F32),
-            pltpu.VMEM((2, NZ, 4, 128), F32),
+            pltpu.VMEM((NZ, 4, 128), F32),
             pltpu.VMEM((NZ, 2, 256, 256), BF16),
             pltpu.VMEM((2, 256, 256), BF16),
-            pltpu.VMEM((NY, 2, NZ, 4, 128), F32),
-            pltpu.VMEM((NZ, 2, 4, 128), F32),
-            pltpu.VMEM((NZ, 2, 4, 128), F32),
-            pltpu.VMEM((NZ, 2, 4, 128), F32),
+            pltpu.VMEM((NY, NZ, 4, 128), F32),
+            pltpu.VMEM((NZ, NZ, 4, 128), F32),
+            pltpu.VMEM((NZ, 4, 128), F32),
             pltpu.VMEM((NY, NZ, 2, 32, 256), BF16),
             pltpu.VMEM((NY - 1, NZ, 2, 32, 256), BF16),
             pltpu.VMEM((NZ, 2, 32, 256), BF16),
@@ -510,10 +557,10 @@
             pltpu.VMEM((NZ, NY, 2, 32, 256), BF16),
             pltpu.VMEM((256, 128), BF16),
             pltpu.VMEM((256, 128), BF16),
-            DMA((7,)), DMA((3, NY)), DMA((3, NY)), *y_pair, *y_pair,
-            *z_pair, DMA((2, NZ)), DMA((2, NZ)),
-            *z_pair, *zy_pair, *z_pair, *zy_pair,
-            *y_pair, *z_pair, *z_pair, *zy_pair, *z_pair, DMA, DMA,
+            DMA((8,)), DMA((4, NY)), DMA((4, NY)), *y_pair, *y_pair,
+            DMA((2, NZ)), DMA((2, NZ)), DMA((2, NZ)), DMA((2, NZ)),
+            *z_pair, *zy_pair, DMA((2, NZ)), DMA((2, NZ)), DMA((2, NZ, NY - 1)), DMA((2, NZ, NY - 1)),
+            *y_pair, *z_pair, *zy_pair, *z_pair, DMA, DMA,
         ],
         compiler_params=pltpu.CompilerParams(
             collective_id=0, has_side_effects=True, vmem_limit_bytes=56 * 1024 * 1024
@@ -521,64 +568,102 @@
     )(*operands)
 
 
-def insert_kernel(length, accepted, k_ref, v_ref, new_ref, ko_ref, vo_ref, kn, vn, kt, vt):
-    b = pl.program_id(0)
-    offset = (lax.axis_index("kv_0") * NY + lax.axis_index("kv_1")) * 32
-    at = jnp.clip(length[b] + accepted[b] - offset + 16, 0, 48)
-    for i in range(NY):
-        for v in range(4):
-            kn[pl.ds(i * 4 + v, 16, stride=16), :] = new_ref[0, i, 0, :, v * 128:(v + 1) * 128].astype(F32)
-        for v in range(4):
-            h, half = v // 2, v % 2
-            vn[half, pl.ds(i * 2 + h, 16, stride=8), :] = new_ref[0, i, 0, :, 512 + v * 128:640 + v * 128].astype(F32)
-    kt[16:48] = k_ref[0]
-    vt[16:48] = v_ref[0]
-    kt[pl.ds(at, 16)] = kn[...].reshape(16, 16, 128).astype(BF16)
-    for half in range(2):
-        vt[pl.ds(at, 16), :, half * 128:(half + 1) * 128] = vn[half].reshape(16, 8, 128).astype(BF16)
-    ko_ref[0] = kt[16:48]
-    vo_ref[0] = vt[16:48]
-
-
-def insert(length, accepted, keys, values, new):
-    def spec(*shape):
-        return pl.BlockSpec((1, *shape), lambda b, *_: (b, 0, 0, 0))
-
+def insert_kernel(length, accepted, k_in, v_in, kg, vg, ko, vo, kt, vt, ins, new, outs):
+    z, y, _ = places()
+    offset = (z * NY + y) * 32
+
+    def load(b):
+        return (
+            pltpu.make_async_copy(k_in.at[b], kt.at[b, 16:48], ins.at[0, b]),
+            pltpu.make_async_copy(v_in.at[b], vt.at[b, 16:48], ins.at[1, b]),
+        )
+
+    def place(b):
+        at = pl.ds(jnp.clip(length[b] + accepted[b] - offset + 16, 0, 48), 16)
+        rows = pl.ds((b % 2) * 16, 16)
+        return [
+            pltpu.make_async_copy(kg.at[b // 2, i, rows], kt.at[b, at, i], new.at[0, b, i]) for i in range(NY)
+        ] + [
+            pltpu.make_async_copy(vg.at[b // 2, i, rows], vt.at[b, at, :, i], new.at[1, b, i]) for i in range(NY)
+        ]
+
+    def store(b):
+        return (
+            pltpu.make_async_copy(kt.at[b, 16:48], ko.at[b], outs.at[0, b]),
+            pltpu.make_async_copy(vt.at[b, 16:48], vo.at[b], outs.at[1, b]),
+        )
+
+    def each(body):
+        def step(b, carry):
+            body(b)
+            return carry
+
+        lax.fori_loop(0, 16, step, 0)
+
+    def act(copies, name):
+        for copy in copies:
+            getattr(copy, name)()
+
+    each(lambda b: act(load(b), "start"))
+
+    @pl.when(z >= NZ // 2)
+    def _():
+        def body(b):
+            act(load(b), "wait")
+            act(place(b), "start")
+
+        each(body)
+
+        def body(b):
+            act(place(b), "wait")
+            act(store(b), "start")
+
+        each(body)
+
+    @pl.when(z < NZ // 2)
+    def _():
+        def body(b):
+            act(load(b), "wait")
+            act(store(b), "start")
+
+        each(body)
+
+    each(lambda b: act(store(b), "wait"))
+
+
+def insert(length, accepted, keys, values, new_keys, new_values):
+    smem, anywhere = pl.BlockSpec(memory_space=pltpu.SMEM), pl.BlockSpec(memory_space=pltpu.HBM)
     return pl.pallas_call(
         insert_kernel,
         name="insert",
-        grid_spec=pltpu.PrefetchScalarGridSpec(
-            num_scalar_prefetch=2,
-            grid=(16,),
-            in_specs=[
-                spec(32, 16, 128), spec(32, 8, 256),
-                pl.BlockSpec((1, NY, 1, 16, 1024), lambda b, *_: (b // 2, 0, b % 2, 0, 0)),
-            ],
-            out_specs=(spec(32, 16, 128), spec(32, 8, 256)),
-            scratch_shapes=[
-                pltpu.VMEM((256, 128), F32), pltpu.VMEM((2, 128, 128), F32),
-                pltpu.VMEM((64, 16, 128), BF16), pltpu.VMEM((64, 8, 256), BF16),
-            ],
+        in_specs=[smem] * 2 + [anywhere] * 4,
+        out_specs=(anywhere, anywhere),
+        scratch_shapes=[
+            pltpu.VMEM((16, 64, NY, 4, 128), BF16), pltpu.VMEM((16, 64, 2, NY, 2, 128), BF16),
+            DMA((2, 16)), DMA((2, 16, NY)), DMA((2, 16)),
+        ],
+        out_shape=(
+            jax.ShapeDtypeStruct((16, 32, NY, 4, 128), BF16),
+            jax.ShapeDtypeStruct((16, 32, 2, NY, 2, 128), BF16),
         ),
-        out_shape=(
-            jax.ShapeDtypeStruct((16, 32, 16, 128), BF16),
-            jax.ShapeDtypeStruct((16, 32, 8, 256), BF16),
-        ),
-    )(length, accepted, keys, values, new)
+        compiler_params=pltpu.CompilerParams(vmem_limit_bytes=62 * 1024 * 1024),
+    )(length, accepted, keys, values, new_keys, new_values)
 
 
 def per_device(tokens, in_gain, query_weight, key_weight, value_weight, out_weight, lambdas, sub_gain,
                key_cache, value_cache, cache_len, accepted, parents):
     frequency = np.float32(10000.0) ** (-np.arange(64, dtype=np.float32) / np.float32(64))
     frequency = jnp.asarray(np.concatenate([frequency, frequency])[None, :])
-    output, new = layer(
+    output, new_keys, new_values = layer(
         cache_len, accepted, lambdas, parents, tokens.reshape(256, 128), in_gain.reshape(1, 128),
-        sub_gain.reshape(1, 256), frequency, query_weight, key_weight, value_weight,
+        sub_gain, frequency, query_weight, key_weight, value_weight,
         key_cache.reshape(16, 512, 128), value_cache.reshape(16, 256, 256), out_weight,
     )
+    values = value_cache.reshape(16, 32, NY, 2, 2, 128).transpose(0, 1, 4, 2, 3, 5)
     key_out, value_out = insert(
-        cache_len, accepted, key_cache.reshape(16, 32, 16, 128), value_cache, new.reshape(NZ, NY, 2, 16, 1024)
+        cache_len, accepted, key_cache.reshape(16, 32, NY, 4, 128), values, new_keys, new_values
     )
+    value_out = value_out.transpose(0, 1, 3, 4, 2, 5).reshape(value_cache.shape)
     return output.reshape(16, 16, 64), key_out.reshape(key_cache.shape), value_out
 
 

time: 123 us -> 111 us (0.902)
  the two profiles are of different devices: /device:TPU:135 before, /device:TPU:161 now
where the time goes in v3:
time: 111 us; the launch traced here: 110 us
  Pallas kernels  109 us (98%)
    pallas_call x1, Pallas kernels, layer(): pl.pallas_call(layer_kernel, name='layer', out_shape=(jax.ShapeDtypeStruc...  102 us
    pallas_call x1, Pallas kernels, insert(): pl.pallas_call(insert_kernel, name='insert', in_specs=[smem] * 2 + [anywh...  6.77 us

profile of v3, /device:TPU:161, one launch (start us, length us, event | category | flops | bytes accessed | tf_op | source)
XLA Modules:
  0.0 110.3 jit_solution(10161710826913668998)
XLA Ops:
  0.6 102.2 %layer.1 = (bf16[256,64]{1,0:T(8,128)(2,1)}, bf16[8,4,32,4,128]{4,3,2,1,0:T(4,128)(2,1)}, bf16[8,4,32,2,2,128]{5,4,3,2,1,0:T(2,128)(2,1)}) custom-call(s32[16]{0:T(128)} %length.3, s32[16]{0:T(128)} %accepted.3, f32[8]{0:T(128)} %lambdas.1, s32[16,16]{1,0:T(8,128)} %parents.1, bf16[256,128]{1,0:T(8,128)(2,1)} %bitcast.17, bf16[1,128]{1,0:T(2,128)(2,1)} %bitcast.19, ...), custom_call_target="tpu_custom_call" | custom-call | tf_op jit(solution)/shard_map/layer/pallas_call | solution.py:514
  102.9 0.0 copy-start
  102.9 6.8 %insert.1 = (bf16[16,32,4,4,128]{4,3,2,1,0:T(4,128)(2,1)}, bf16[16,32,2,4,2,128]{5,4,3,2,1,0:T(2,128)(2,1)}) custom-call(s32[16]{0:T(128)} %length.3, s32[16]{0:T(128)} %accepted.3, bf16[16,32,4,4,128]{4,3,2,1,0:T(4,128)(2,1)} %bitcast.14, bf16[16,32,2,4,2,128]{5,4,3,2,1,0:T(2,128)(2,1)} %bitcast.16, bf16[8,4,32,4,128]{4,3,2,1,0:T(4,128)(2,1)} %get-tuple-element.9.kg, ...), custom_call_target="tpu_custom_call" | custom-call | tf_op jit(solution)/shard_map/insert/pallas_call | solution.py:636
  109.7 0.0 copy-done
  109.7 0.6 copy.18
Async XLA Ops:
  102.9 6.8 %copy-start = (bf16[256,64]{1,0:T(8,128)(2,1)S(1)}, bf16[256,64]{1,0:T(8,128)(2,1)}, u32[]{:S(2)}) copy-start(bf16[256,64]{1,0:T(8,128)(2,1)} %get-tuple-element.8) | copy-start | bytes 98308

commit v4 on v3

--- a/solution.py
+++ b/solution.py
@@ -22,6 +22,7 @@
 DMA = pltpu.SemaphoreType.DMA
 Z_STEPS = (1, 7, 2, 6, 3, 5, 4)
 Y_STEPS = (1, 3, 2)
+FAR_FIRST = (4, 3, 5, 2, 6, 1, 7)
 
 
 def places():
@@ -191,12 +192,14 @@
         return remote(pkv.at[m, to], zkv.at[m, d], ks.at[m, d], kr.at[m, d], kv_0=to)
 
     pq0[:, :, 0:256] = product(0)
-    for d in Z_STEPS:
+    for d in FAR_FIRST:
         q_copy(0, d).start()
     pq1[...] = product(1)
-    for d in Z_STEPS:
+    for d in FAR_FIRST:
         q_copy(1, d).start()
     pkv[0] = product(2)
+    for d in FAR_FIRST:
+        kv_copy(0, d).start()
 
     totals = []
     for i in range(2):
@@ -219,13 +222,7 @@
     q_start, q_hand_on, q_arrived, q_end = gather_2d(qg, z, y, azs, azr, ays, ayr)
     q_start()
     for d in Z_STEPS:
-        kv_copy(0, d).start()
-    for d in Z_STEPS:
         q_hand_on(d)
-    pkv[1] = product(3)
-    for d in Z_STEPS:
-        kv_copy(1, d).start()
-
     def finished(m):
         total = pkv[m, z].astype(F32)
         for d in Z_STEPS:
@@ -286,6 +283,13 @@
             for k in (0, *Z_STEPS):
                 up_y(m, k, (1, 3)[m]).wait_recv()
                 relay(m, k).start()
+
+    finished(0)
+    knew[...] = turn[0].astype(BF16).reshape(32, 4, 128)
+    go_up(0)
+    pkv[1] = product(3)
+    for d in Z_STEPS:
+        kv_copy(1, d).start()
 
     loads[0].wait()
     loads[1].wait()
@@ -327,17 +331,10 @@
             acc[zc, s] = contract(chance, vc[b], ((0,), (0,))).astype(BF16)
         return carry
 
-    lax.fori_loop(0, NZ - 2, attend, 0)
-    finished(0)
-    knew[...] = turn[0].astype(BF16).reshape(32, 4, 128)
-    go_up(0)
-
-    lax.fori_loop(NZ - 2, NZ, attend, 0)
+    lax.fori_loop(0, NZ, attend, 0)
     q_end()
-    finished(1)
-    vnew[...] = turn[1].astype(BF16).reshape(32, 2, 2, 128)
-    go_up(1)
-
+
+    weights = []
     head_row = 2 * y + lax.broadcasted_iota(jnp.int32, (32, 128), 0) // 16
     head_lane = lax.broadcasted_iota(jnp.int32, (32, 128), 1) // 16
     for s in range(2):
@@ -345,7 +342,6 @@
         keys = jnp.concatenate(
             [kvown[rows, (h * 2 + m) * 128:(h * 2 + m + 1) * 128] for m in range(2) for h in range(2)], axis=0
         )
-        values = jnp.concatenate([kvown[rows, 512:768], kvown[rows, 768:1024]], axis=0)
         both = contract(keys, queries_of(z, s), ((1,), (1,)))
         live = (head_row == head_lane) & (jnp.concatenate([seen[s], seen[s]], axis=0) > 0.5)
         chance = []
@@ -356,7 +352,7 @@
             sx[0, 2 * s + m:2 * s + m + 1] = peak
             sx[1, 2 * s + m:2 * s + m + 1] = jnp.sum(grown, axis=0, keepdims=True)
             chance.append(grown)
-        accx[s] = contract(jnp.concatenate(chance, axis=1).astype(BF16), values, ((0,), (0,))).astype(BF16)
+        weights.append(jnp.concatenate(chance, axis=1).astype(BF16))
     def log_sum(peak, total):
         return peak + jnp.log(jnp.maximum(total, 1e-30))
 
@@ -372,6 +368,7 @@
 
     for e in Y_STEPS:
         st_copy(e).start()
+    hand_up(0)
     parts = [mst[...]]
     for e in Y_STEPS:
         st_copy(e).wait_recv()
@@ -381,9 +378,16 @@
     def st_z(d):
         return remote(zst.at[0], zst.at[d], s2.at[d], r2.at[d], kv_0=(z + d) % NZ)
 
-    for d in Z_STEPS:
+    for d in FAR_FIRST:
         st_z(d).start()
-    hand_up(0)
+    finished(1)
+    vnew[...] = turn[1].astype(BF16).reshape(32, 2, 2, 128)
+    go_up(1)
+    for s in range(2):
+        rows = slice(s * 16, (s + 1) * 16)
+        values = jnp.concatenate([kvown[rows, 512:768], kvown[rows, 768:1024]], axis=0)
+        accx[s] = contract(weights[s], values, ((0,), (0,))).astype(BF16)
+    hand_over(0)
     row = lax.broadcasted_iota(jnp.int32, (128, 128), 0)
     lane = lax.broadcasted_iota(jnp.int32, (128, 128), 1)
     same = row == lane
@@ -442,7 +446,6 @@
 
     lax.fori_loop(1, NZ + 1, sums, 0)
     hand_up(1)
-    hand_over(0)
     total = zsum[z].astype(F32)
     for d in range(1, NZ):
         send_z(d).wait_recv()
@@ -572,10 +575,13 @@
     z, y, _ = places()
     offset = (z * NY + y) * 32
 
-    def load(b):
+    def group(g):
+        return pl.ds(g * 4, 4)
+
+    def load(g):
         return (
-            pltpu.make_async_copy(k_in.at[b], kt.at[b, 16:48], ins.at[0, b]),
-            pltpu.make_async_copy(v_in.at[b], vt.at[b, 16:48], ins.at[1, b]),
+            pltpu.make_async_copy(k_in.at[group(g)], kt.at[group(g), 16:48], ins.at[0, g]),
+            pltpu.make_async_copy(v_in.at[group(g)], vt.at[group(g), 16:48], ins.at[1, g]),
         )
 
     def place(b):
@@ -587,48 +593,38 @@
             pltpu.make_async_copy(vg.at[b // 2, i, rows], vt.at[b, at, :, i], new.at[1, b, i]) for i in range(NY)
         ]
 
-    def store(b):
+    def store(g):
         return (
-            pltpu.make_async_copy(kt.at[b, 16:48], ko.at[b], outs.at[0, b]),
-            pltpu.make_async_copy(vt.at[b, 16:48], vo.at[b], outs.at[1, b]),
+            pltpu.make_async_copy(kt.at[group(g), 16:48], ko.at[group(g)], outs.at[0, g]),
+            pltpu.make_async_copy(vt.at[group(g), 16:48], vo.at[group(g)], outs.at[1, g]),
         )
-
-    def each(body):
-        def step(b, carry):
-            body(b)
-            return carry
-
-        lax.fori_loop(0, 16, step, 0)
 
     def act(copies, name):
         for copy in copies:
             getattr(copy, name)()
 
-    each(lambda b: act(load(b), "start"))
+    for g in range(4):
+        act(load(g), "start")
 
     @pl.when(z >= NZ // 2)
     def _():
-        def body(b):
-            act(load(b), "wait")
-            act(place(b), "start")
-
-        each(body)
-
-        def body(b):
-            act(place(b), "wait")
-            act(store(b), "start")
-
-        each(body)
+        for g in range(4):
+            act(load(g), "wait")
+            for b in range(4 * g, 4 * g + 4):
+                act(place(b), "start")
+        for g in range(4):
+            for b in range(4 * g, 4 * g + 4):
+                act(place(b), "wait")
+            act(store(g), "start")
 
     @pl.when(z < NZ // 2)
     def _():
-        def body(b):
-            act(load(b), "wait")
-            act(store(b), "start")
-
-        each(body)
-
-    each(lambda b: act(store(b), "wait"))
+        for g in range(4):
+            act(load(g), "wait")
+            act(store(g), "start")
+
+    for g in range(4):
+        act(store(g), "wait")
 
 
 def insert(length, accepted, keys, values, new_keys, new_values):
@@ -640,7 +636,7 @@
         out_specs=(anywhere, anywhere),
         scratch_shapes=[
             pltpu.VMEM((16, 64, NY, 4, 128), BF16), pltpu.VMEM((16, 64, 2, NY, 2, 128), BF16),
-            DMA((2, 16)), DMA((2, 16, NY)), DMA((2, 16)),
+            DMA((2, 4)), DMA((2, 16, NY)), DMA((2, 4)),
         ],
         out_shape=(
             jax.ShapeDtypeStruct((16, 32, NY, 4, 128), BF16),

time: 111 us -> 103 us (0.928)
  the two profiles are of different devices: /device:TPU:161 before, /device:TPU:135 now
where the time goes in v4:
time: 103 us
  Pallas kernels  101 us (98%)
    pallas_call x1, Pallas kernels, layer(): pl.pallas_call(layer_kernel, name='layer', out_shape=(jax.ShapeDtypeStruc...  94.9 us
    pallas_call x1, Pallas kernels, insert(): pl.pallas_call(insert_kernel, name='insert', in_specs=[smem] * 2 + [anywh...  6.47 us

profile of v4, /device:TPU:135, one launch (start us, length us, event | category | flops | bytes accessed | tf_op | source)
XLA Modules:
  0.0 102.6 jit_solution(17437396285862417781)
XLA Ops:
  0.6 94.9 %layer.1 = (bf16[256,64]{1,0:T(8,128)(2,1)}, bf16[8,4,32,4,128]{4,3,2,1,0:T(4,128)(2,1)}, bf16[8,4,32,2,2,128]{5,4,3,2,1,0:T(2,128)(2,1)}) custom-call(s32[16]{0:T(128)} %length.3, s32[16]{0:T(128)} %accepted.3, f32[8]{0:T(128)} %lambdas.1, s32[16,16]{1,0:T(8,128)} %parents.1, bf16[256,128]{1,0:T(8,128)(2,1)} %bitcast.17, bf16[1,128]{1,0:T(2,128)(2,1)} %bitcast.19, ...), custom_call_target="tpu_custom_call" | custom-call | tf_op jit(solution)/shard_map/layer/pallas_call | solution.py:517
  95.5 0.0 copy-start
  95.5 6.5 %insert.1 = (bf16[16,32,4,4,128]{4,3,2,1,0:T(4,128)(2,1)}, bf16[16,32,2,4,2,128]{5,4,3,2,1,0:T(2,128)(2,1)}) custom-call(s32[16]{0:T(128)} %length.3, s32[16]{0:T(128)} %accepted.3, bf16[16,32,4,4,128]{4,3,2,1,0:T(4,128)(2,1)} %bitcast.14, bf16[16,32,2,4,2,128]{5,4,3,2,1,0:T(2,128)(2,1)} %bitcast.16, bf16[8,4,32,4,128]{4,3,2,1,0:T(4,128)(2,1)} %get-tuple-element.9.kg, ...), custom_call_target="tpu_custom_call" | custom-call | tf_op jit(solution)/shard_map/insert/pallas_call | solution.py:632
  102.0 0.0 copy-done
  102.0 0.6 copy.18
Async XLA Ops:
  95.5 6.5 %copy-start = (bf16[256,64]{1,0:T(8,128)(2,1)S(1)}, bf16[256,64]{1,0:T(8,128)(2,1)}, u32[]{:S(2)}) copy-start(bf16[256,64]{1,0:T(8,128)(2,1)} %get-tuple-element.8) | copy-start | bytes 98308

commit v5 on v4

--- a/solution.py
+++ b/solution.py
@@ -47,7 +47,9 @@
     pl.semaphore_wait(barrier, NZ - 1 + NY - 1 + int(with_tp))
 
 
-def gather_2d(buf, z, y, zs, zr, ys, yr):
+def gather_2d(buf, z, y, zs, zr, ys, yr, relayed):
+    direct = (1, 3) if relayed else Y_STEPS
+
     def z_copy(d):
         return remote(buf.at[z, y], buf.at[z, y], zs.at[d], zr.at[d], kv_0=(z + d) % NZ)
 
@@ -55,29 +57,46 @@
         row = (z + NZ - k) % NZ
         return remote(buf.at[row, y], buf.at[row, y], ys.at[k, e - 1], yr.at[k, e - 1], kv_1=(y + e) % NY)
 
+    def y_relay(k, half):
+        at, to = (y + (3, 1)[half]) % NY, (y + (1, 3)[half]) % NY
+        block = buf.at[(z + NZ - k) % NZ, at, half]
+        return remote(block, block, ys.at[k, 1 + 2 * half], yr.at[k, 1 + 2 * half], kv_1=to)
+
     def start():
         for d in Z_STEPS:
             z_copy(d).start()
-        for e in Y_STEPS:
+        for e in direct:
             y_copy(0, e).start()
 
     def hand_on(d):
         z_copy(d).wait_recv()
-        for e in Y_STEPS:
+        for e in direct:
             y_copy(d, e).start()
 
     def arrived(k):
-        for e in Y_STEPS:
+        for e in direct:
             y_copy(k, e).wait_recv()
+
+    def hand_over(k):
+        arrived(k)
+        for half in range(2):
+            y_relay(k, half).start()
+
+    def handed_over(k):
+        for half in range(2):
+            y_relay(k, half).wait_recv()
 
     def end():
         for d in Z_STEPS:
             z_copy(d).wait_send()
         for k in (0, *Z_STEPS):
-            for e in Y_STEPS:
+            for e in direct:
                 y_copy(k, e).wait_send()
-
-    return start, hand_on, arrived, end
+            if relayed:
+                for half in range(2):
+                    y_relay(k, half).wait_send()
+
+    return start, hand_on, arrived, hand_over, handed_over, end
 
 
 def contract(a, b, dims):
@@ -219,10 +238,8 @@
         block = turned(totals[v // 2][:, v % 2 * 128:v % 2 * 128 + 128] * scale).astype(BF16)
         qg[z, y, 0, :, cols] = block[0:16]
         qg[z, y, 1, :, cols] = block[16:32]
-    q_start, q_hand_on, q_arrived, q_end = gather_2d(qg, z, y, azs, azr, ays, ayr)
+    q_start, q_hand_on, q_arrived, _, _, q_end = gather_2d(qg, z, y, azs, azr, ays, ayr, False)
     q_start()
-    for d in Z_STEPS:
-        q_hand_on(d)
     def finished(m):
         total = pkv[m, z].astype(F32)
         for d in Z_STEPS:
@@ -250,8 +267,8 @@
     own_up = [pltpu.make_async_copy(pairs[m][0], pairs[m][1].at[z, y], ls.at[6 + m]) for m in range(2)]
 
     def relay(m, k):
-        at, to = (z + NZ - k) % NZ, (y + (1, 3)[m]) % NY
-        block = pairs[m][1].at[at, (y + (3, 1)[m]) % NY]
+        at, to = (z + NZ - k) % NZ, (y + (1, 3)[k % 2]) % NY
+        block = pairs[m][1].at[at, (y + (3, 1)[k % 2]) % NY]
         return remote(block, block, kys.at[m, k, 1], kyr.at[m, k, 1], kv_1=to)
 
     def to_upper(m, act):
@@ -281,18 +298,8 @@
         @pl.when(upper)
         def _():
             for k in (0, *Z_STEPS):
-                up_y(m, k, (1, 3)[m]).wait_recv()
+                up_y(m, k, (1, 3)[k % 2]).wait_recv()
                 relay(m, k).start()
-
-    finished(0)
-    knew[...] = turn[0].astype(BF16).reshape(32, 4, 128)
-    go_up(0)
-    pkv[1] = product(3)
-    for d in Z_STEPS:
-        kv_copy(1, d).start()
-
-    loads[0].wait()
-    loads[1].wait()
 
     def queries_of(zc, s):
         return jnp.concatenate(
@@ -331,7 +338,21 @@
             acc[zc, s] = contract(chance, vc[b], ((0,), (0,))).astype(BF16)
         return carry
 
-    lax.fori_loop(0, NZ, attend, 0)
+    for d in Z_STEPS[:4]:
+        q_hand_on(d)
+    loads[0].wait()
+    loads[1].wait()
+    attend(jnp.int32(0), 0)
+    for d in Z_STEPS[4:]:
+        q_hand_on(d)
+    finished(0)
+    knew[...] = turn[0].astype(BF16).reshape(32, 4, 128)
+    go_up(0)
+    pkv[1] = product(3)
+    for d in Z_STEPS:
+        kv_copy(1, d).start()
+
+    lax.fori_loop(1, NZ, attend, 0)
     q_end()
 
     weights = []
@@ -452,14 +473,35 @@
         total += zbuf[d].astype(F32)
     norm = total * lax.rsqrt(jnp.mean(total * total, axis=-1, keepdims=True) + 1e-05)
     mg[z, y] = (norm * sub[...].astype(F32).reshape(1, 256) * LAMBDA_SCALE).astype(BF16)
-    m_start, m_hand_on, m_arrived, m_end = gather_2d(mg, z, y, azs, azr, ays, ayr)
-    m_start()
-    for d in Z_STEPS:
-        m_hand_on(d)
+    m_start, m_hand_on, m_arrived, _, _, m_end = gather_2d(mg, z, y, azs, azr, ays, ayr, False)
+    r_start, r_hand_on, _, r_hand_over, r_handed_over, r_end = gather_2d(mg, z, y, azs, azr, ays, ayr, True)
+    @pl.when(upper)
+    def _():
+        r_start()
+        for d in Z_STEPS:
+            r_hand_on(d)
+        for k in (0, *Z_STEPS):
+            r_hand_over(k)
+
+    @pl.when(z < NZ // 2)
+    def _():
+        m_start()
+        for d in Z_STEPS:
+            m_hand_on(d)
+
     hand_over(1)
     loads[2].wait()
-    for k in (0, *Z_STEPS):
-        m_arrived(k)
+
+    @pl.when(upper)
+    def _():
+        for k in (0, *Z_STEPS):
+            r_handed_over(k)
+
+    @pl.when(z < NZ // 2)
+    def _():
+        for k in (0, *Z_STEPS):
+            m_arrived(k)
+
     result = jnp.zeros((256, 128), F32)
     for h in range(8):
         i, k = h // 2, h % 2
@@ -488,7 +530,8 @@
         st_z(d).wait_send()
         send_z(d).wait_send()
 
-    m_end()
+    pl.when(upper)(r_end)
+    pl.when(z < NZ // 2)(m_end)
     for m in range(2):
         to_upper(m, lambda copy: copy.wait_send())
 
@@ -505,7 +548,7 @@
             for k in (0, *Z_STEPS):
                 up_y(m, k, 1).wait_send()
                 up_y(m, k, 3).wait_send()
-                up_y(m, k, (3, 1)[m]).wait_recv()
+                up_y(m, k, (3, 1)[k % 2]).wait_recv()
                 relay(m, k).wait()
 
 
@@ -562,7 +605,7 @@
             pltpu.VMEM((256, 128), BF16),
             DMA((8,)), DMA((4, NY)), DMA((4, NY)), *y_pair, *y_pair,
             DMA((2, NZ)), DMA((2, NZ)), DMA((2, NZ)), DMA((2, NZ)),
-            *z_pair, *zy_pair, DMA((2, NZ)), DMA((2, NZ)), DMA((2, NZ, NY - 1)), DMA((2, NZ, NY - 1)),
+            *z_pair, DMA((NZ, NY)), DMA((NZ, NY)), DMA((2, NZ)), DMA((2, NZ)), DMA((2, NZ, NY - 1)), DMA((2, NZ, NY - 1)),
             *y_pair, *z_pair, *zy_pair, *z_pair, DMA, DMA,
         ],
         compiler_params=pltpu.CompilerParams(

time: 103 us -> 100 us (0.971); the launches traced: 103 us -> 98.6 us
  Pallas kernels: 101 us -> 97.3 us
    pallas_call x1, Pallas kernels: 94.9 us -> 90.8 us  [layer(): pl.pallas_call(layer_kernel, name='layer', out_shape=(jax.ShapeDtypeStruc...]
where the time goes in v5:
time: 100 us; the launch traced here: 98.6 us
  Pallas kernels  97.3 us (97%)
    pallas_call x1, Pallas kernels, layer(): pl.pallas_call(layer_kernel, name='layer', out_shape=(jax.ShapeDtypeStruc...  90.8 us
    pallas_call x1, Pallas kernels, insert(): pl.pallas_call(insert_kernel, name='insert', in_specs=[smem] * 2 + [anywh...  6.47 us

profile of v5, /device:TPU:135, one launch (start us, length us, event | category | flops | bytes accessed | tf_op | source)
XLA Modules:
  0.0 98.6 jit_solution(1714205909142710411)
XLA Ops:
  0.6 90.8 %layer.1 = (bf16[256,64]{1,0:T(8,128)(2,1)}, bf16[8,4,32,4,128]{4,3,2,1,0:T(4,128)(2,1)}, bf16[8,4,32,2,2,128]{5,4,3,2,1,0:T(2,128)(2,1)}) custom-call(s32[16]{0:T(128)} %length.3, s32[16]{0:T(128)} %accepted.3, f32[8]{0:T(128)} %lambdas.1, s32[16,16]{1,0:T(8,128)} %parents.1, bf16[256,128]{1,0:T(8,128)(2,1)} %bitcast.17, bf16[1,128]{1,0:T(2,128)(2,1)} %bitcast.19, ...), custom_call_target="tpu_custom_call" | custom-call | tf_op jit(solution)/shard_map/layer/pallas_call | solution.py:560
  91.4 0.0 copy-start
  91.4 6.5 %insert.1 = (bf16[16,32,4,4,128]{4,3,2,1,0:T(4,128)(2,1)}, bf16[16,32,2,4,2,128]{5,4,3,2,1,0:T(2,128)(2,1)}) custom-call(s32[16]{0:T(128)} %length.3, s32[16]{0:T(128)} %accepted.3, bf16[16,32,4,4,128]{4,3,2,1,0:T(4,128)(2,1)} %bitcast.14, bf16[16,32,2,4,2,128]{5,4,3,2,1,0:T(2,128)(2,1)} %bitcast.16, bf16[8,4,32,4,128]{4,3,2,1,0:T(4,128)(2,1)} %get-tuple-element.9.kg, ...), custom_call_target="tpu_custom_call" | custom-call | tf_op jit(solution)/shard_map/insert/pallas_call | solution.py:675
  97.9 0.0 copy-done
  97.9 0.6 copy.18
Async XLA Ops:
  91.4 6.5 %copy-start = (bf16[256,64]{1,0:T(8,128)(2,1)S(1)}, bf16[256,64]{1,0:T(8,128)(2,1)}, u32[]{:S(2)}) copy-start(bf16[256,64]{1,0:T(8,128)(2,1)} %get-tuple-element.8) | copy-start | bytes 98308

commit v6 on v5

--- a/solution.py
+++ b/solution.py
@@ -62,11 +62,12 @@
         block = buf.at[(z + NZ - k) % NZ, at, half]
         return remote(block, block, ys.at[k, 1 + 2 * half], yr.at[k, 1 + 2 * half], kv_1=to)
 
-    def start():
-        for d in Z_STEPS:
+    def start(steps=Z_STEPS, along_y=True):
+        for d in steps:
             z_copy(d).start()
-        for e in direct:
-            y_copy(0, e).start()
+        if along_y:
+            for e in direct:
+                y_copy(0, e).start()
 
     def hand_on(d):
         z_copy(d).wait_recv()
@@ -217,8 +218,6 @@
     for d in FAR_FIRST:
         q_copy(1, d).start()
     pkv[0] = product(2)
-    for d in FAR_FIRST:
-        kv_copy(0, d).start()
 
     totals = []
     for i in range(2):
@@ -239,7 +238,10 @@
         qg[z, y, 0, :, cols] = block[0:16]
         qg[z, y, 1, :, cols] = block[16:32]
     q_start, q_hand_on, q_arrived, _, _, q_end = gather_2d(qg, z, y, azs, azr, ays, ayr, False)
-    q_start()
+    q_start(Z_STEPS[:2])
+    for d in FAR_FIRST:
+        kv_copy(0, d).start()
+    q_start(Z_STEPS[2:], False)
     def finished(m):
         total = pkv[m, z].astype(F32)
         for d in Z_STEPS:
@@ -338,12 +340,12 @@
             acc[zc, s] = contract(chance, vc[b], ((0,), (0,))).astype(BF16)
         return carry
 
-    for d in Z_STEPS[:4]:
+    for d in Z_STEPS[:2]:
         q_hand_on(d)
     loads[0].wait()
     loads[1].wait()
-    attend(jnp.int32(0), 0)
-    for d in Z_STEPS[4:]:
+    lax.fori_loop(0, 3, attend, 0)
+    for d in Z_STEPS[2:]:
         q_hand_on(d)
     finished(0)
     knew[...] = turn[0].astype(BF16).reshape(32, 4, 128)
@@ -352,7 +354,7 @@
     for d in Z_STEPS:
         kv_copy(1, d).start()
 
-    lax.fori_loop(1, NZ, attend, 0)
+    lax.fori_loop(3, NZ, attend, 0)
     q_end()
 
     weights = []

time: 100 us -> 99.6 us (level)
  no operation moved by 1% of the time
where the time goes in v6:
time: 99.6 us; the launch traced here: 98.3 us
  Pallas kernels  97 us (97%)
    pallas_call x1, Pallas kernels, layer(): pl.pallas_call(layer_kernel, name='layer', out_shape=(jax.ShapeDtypeStruc...  90.5 us
    pallas_call x1, Pallas kernels, insert(): pl.pallas_call(insert_kernel, name='insert', in_specs=[smem] * 2 + [anywh...  6.47 us

profile of v6, /device:TPU:135, one launch (start us, length us, event | category | flops | bytes accessed | tf_op | source)
XLA Modules:
  0.0 98.3 jit_solution(8527338473282274120)
XLA Ops:
  0.6 90.5 %layer.1 = (bf16[256,64]{1,0:T(8,128)(2,1)}, bf16[8,4,32,4,128]{4,3,2,1,0:T(4,128)(2,1)}, bf16[8,4,32,2,2,128]{5,4,3,2,1,0:T(2,128)(2,1)}) custom-call(s32[16]{0:T(128)} %length.3, s32[16]{0:T(128)} %accepted.3, f32[8]{0:T(128)} %lambdas.1, s32[16,16]{1,0:T(8,128)} %parents.1, bf16[256,128]{1,0:T(8,128)(2,1)} %bitcast.17, bf16[1,128]{1,0:T(2,128)(2,1)} %bitcast.19, ...), custom_call_target="tpu_custom_call" | custom-call | tf_op jit(solution)/shard_map/layer/pallas_call | solution.py:562
  91.2 0.0 copy-start
  91.2 6.5 %insert.1 = (bf16[16,32,4,4,128]{4,3,2,1,0:T(4,128)(2,1)}, bf16[16,32,2,4,2,128]{5,4,3,2,1,0:T(2,128)(2,1)}) custom-call(s32[16]{0:T(128)} %length.3, s32[16]{0:T(128)} %accepted.3, bf16[16,32,4,4,128]{4,3,2,1,0:T(4,128)(2,1)} %bitcast.14, bf16[16,32,2,4,2,128]{5,4,3,2,1,0:T(2,128)(2,1)} %bitcast.16, bf16[8,4,32,4,128]{4,3,2,1,0:T(4,128)(2,1)} %get-tuple-element.9.kg, ...), custom_call_target="tpu_custom_call" | custom-call | tf_op jit(solution)/shard_map/insert/pallas_call | solution.py:677
  97.7 0.0 copy-done
  97.7 0.6 copy.18
Async XLA Ops:
  91.2 6.5 %copy-start = (bf16[256,64]{1,0:T(8,128)(2,1)S(1)}, bf16[256,64]{1,0:T(8,128)(2,1)}, u32[]{:S(2)}) copy-start(bf16[256,64]{1,0:T(8,128)(2,1)} %get-tuple-element.8) | copy-start | bytes 98308
